TPU v7x, 32 devices: a whole 2x2x4 slice. The times are simulated.
32 devices in a mesh: ep: 8 (over z, x), tp: 4 (over y, core).
Axes of the slice: x: 2, y: 2, z: 4, core: 2. Of those that a mesh axis runs over, the one named last changes fastest.
Arguments:
- tokens: bfloat16 [1024, 2048], P('ep'), may hold values from -6 to 6
- cotangent: bfloat16 [1024, 2048], P('ep'), may hold values from -1.5 to 1.5
- routes: int32 [1024, 2], P('ep'), may hold values from 0 to 3, all different within a row; in each aligned block of 128 rows (0 to 127, 128 to 255, ...) at most 96 rows name the same one
- router: bfloat16 [2048, 4], replicated, may hold values from -0.125 to 0.125
- w_gate: bfloat16 [8, 2048, 2048], P('ep', None, 'tp'), may hold values from -0.125 to 0.125
- w_up: bfloat16 [8, 2048, 2048], P('ep', None, 'tp'), may hold values from -0.125 to 0.125
- w_down: bfloat16 [8, 2048, 2048], P('ep', 'tp'), may hold values from -0.09375 to 0.09375
Outputs:
- token_grad: bfloat16 [1024, 2048], P('ep', 'tp')
- gate_grad: float32 [1024, 2], P('ep')
- grad_gate: bfloat16 [8, 2048, 2048], P('ep', None, 'tp')
- grad_up: bfloat16 [8, 2048, 2048], P('ep', None, 'tp')
- grad_down: bfloat16 [8, 2048, 2048], P('ep', 'tp')
- router_grad: float32 [2048, 4], P(('ep', 'tp'))
Inputs may be any that keep to these rules, and one draw needn't show every extreme that they name: `routes`: each row names 2 different experts. In the rows of one index of ep (aligned blocks of 128 rows) no expert is named by more than 96 rows, a bound that some block reaches.
All inputs are finite; a program needn't handle non-finite values.
Results may differ from a plain program's by a relative error of at most 0.018.
Values may be sent and summed in bfloat16 or wider, within the bound.
A program may use at most 64 MiB of HBM per device.

v0:
```python
import jax
import jax.numpy as jnp
from jax import lax
from jax.experimental import pallas as pl
from jax.experimental.pallas import tpu as pltpu
from jax.sharding import PartitionSpec as P

BLOCKS = 2
CORES = 2
MESH = pl.DeviceIdType.MESH


def build_slots(block_routes, experts, capacity):
    flat_routes = block_routes.reshape(-1)
    labels = jnp.arange(experts, dtype=jnp.int32)
    hit_mask = (flat_routes[None, :] == labels[:, None]).astype(jnp.int32)
    rank_in = jnp.cumsum(hit_mask, axis=1, dtype=jnp.int32) - 1
    slot_ids = jnp.arange(capacity, dtype=jnp.int32)
    assigned = (hit_mask[:, None, :] == 1) & (rank_in[:, None, :] == slot_ids[None, :, None])
    return assigned.astype(jnp.float32)


def gate_pair(tokens, routes, router, experts):
    logits = jnp.dot(tokens, router, preferred_element_type=jnp.float32)
    labels = jnp.arange(experts, dtype=jnp.int32)
    picked = (routes[:, :, None] == labels[None, None, :]).astype(jnp.float32)
    chosen = jnp.sum(picked * logits[:, None, :], axis=2)
    margin = chosen[:, 0] - chosen[:, 1]
    weights = jnp.stack([jax.nn.sigmoid(margin), jax.nn.sigmoid(-margin)], axis=1)
    return (picked, weights)


def logit_grads(picked, weights, gate_grad):
    lead_grad = weights[:, 0] * weights[:, 1] * (gate_grad[:, 0] - gate_grad[:, 1])
    pair_grad = jnp.stack([lead_grad, -lead_grad], axis=1)
    return jnp.sum(picked * pair_grad[:, :, None], axis=1)


def expert_grads(rows_in, cot_in, gate_in, gate_weight, up_weight, down_weight):
    pre_gate = jnp.dot(rows_in, gate_weight, preferred_element_type=jnp.float32)
    pre_up = jnp.dot(rows_in, up_weight, preferred_element_type=jnp.float32)
    back_grad = lax.dot_general(
        cot_in, down_weight, (((1,), (1,)), ((), ())), preferred_element_type=jnp.float32
    )
    sig_gate = jax.nn.sigmoid(pre_gate)
    active = pre_gate * sig_gate
    hidden = (active * pre_up).astype(jnp.bfloat16)
    gate_terms = jnp.sum(hidden.astype(jnp.float32) * back_grad, axis=1)
    gate_col = gate_in.astype(jnp.float32)[:, None]
    scaled_back = gate_col * back_grad
    d_gate = (scaled_back * pre_up * sig_gate * (1.0 + pre_gate * (1.0 - sig_gate))).astype(
        jnp.bfloat16
    )
    d_up = (scaled_back * active).astype(jnp.bfloat16)
    scaled_cot = (gate_col * cot_in.astype(jnp.float32)).astype(jnp.bfloat16)
    contract_rows = (((0,), (0,)), ((), ()))
    grad_gate = lax.dot_general(
        rows_in, d_gate, contract_rows, preferred_element_type=jnp.float32
    ).astype(jnp.bfloat16)
    grad_up = lax.dot_general(
        rows_in, d_up, contract_rows, preferred_element_type=jnp.float32
    ).astype(jnp.bfloat16)
    grad_down = lax.dot_general(
        hidden, scaled_cot, contract_rows, preferred_element_type=jnp.float32
    ).astype(jnp.bfloat16)
    return (d_gate, d_up, gate_terms, grad_gate, grad_up, grad_down)


def spread_slabs(packed, experts, slab_count):
    widened = jnp.broadcast_to(packed[:, None], (experts, BLOCKS) + packed.shape[1:])
    return widened.reshape((slab_count,) + packed.shape[1:])


def routed_shards(tokens, cotangent, routes, router, w_gate, w_up, w_down):
    highest = lax.Precision.HIGHEST
    ep_count = lax.axis_size("ep")
    tp_count = lax.axis_size("tp")
    experts = ep_count // BLOCKS
    tok_rows, width = tokens.shape
    top_count = routes.shape[1]
    capacity = 3 * tok_rows * top_count // (2 * experts)
    col_width = width // tp_count
    tp_index = lax.axis_index("tp")
    picked, weights = gate_pair(tokens, routes, router, experts)
    assigned = build_slots(routes, experts, capacity)
    per_token = jnp.sum(assigned.reshape(experts, capacity, tok_rows, top_count), axis=3)
    token_map = per_token.astype(jnp.bfloat16)
    gate_send = weights.astype(jnp.bfloat16)
    gate_slots = jnp.einsum(
        "ecj,j->ec", assigned, gate_send.astype(jnp.float32).reshape(-1), precision=highest
    ).astype(jnp.bfloat16)
    gate_out = spread_slabs(gate_slots, experts, ep_count)

    def pack_rows(source):
        packed = jnp.einsum(
            "ect,td->ecd", token_map, source, preferred_element_type=jnp.float32
        ).astype(jnp.bfloat16)
        return spread_slabs(packed, experts, ep_count)

    tok_part = lax.dynamic_slice_in_dim(tokens, tp_index * col_width, col_width, 1)
    cot_part = lax.dynamic_slice_in_dim(cotangent, tp_index * col_width, col_width, 1)
    recv_part, recv_cot_part, recv_gate = (
        lax.all_to_all(pack_rows(tok_part), "ep", split_axis=0, concat_axis=0, tiled=True),
        lax.all_to_all(pack_rows(cot_part), "ep", split_axis=0, concat_axis=0, tiled=True),
        lax.all_to_all(gate_out, "ep", split_axis=0, concat_axis=0, tiled=True),
    )
    recv_rows, recv_cot = (
        lax.all_gather(recv_part, "tp", axis=2, tiled=True),
        lax.all_gather(recv_cot_part, "tp", axis=2, tiled=True),
    )
    rows_in = recv_rows.reshape(-1, width)
    cot_in = recv_cot.reshape(-1, width)
    gate_in = recv_gate.reshape(-1)
    d_gate, d_up, gate_terms, grad_gate, grad_up, grad_down = expert_grads(
        rows_in, cot_in, gate_in, w_gate[0], w_up[0], w_down[0]
    )
    contract_hidden = (((1,), (1,)), ((), ()))
    partial_dx = lax.dot_general(
        d_gate, w_gate[0], contract_hidden, preferred_element_type=jnp.float32
    )
    partial_dx = partial_dx + lax.dot_general(
        d_up, w_up[0], contract_hidden, preferred_element_type=jnp.float32
    )
    summed_dx = lax.psum_scatter(
        partial_dx.reshape(ep_count, capacity, width).astype(jnp.bfloat16),
        "tp",
        scatter_dimension=2,
        tiled=True,
    ).astype(jnp.float32)
    gate_sums = lax.psum(gate_terms.reshape(ep_count, capacity), "tp")
    back_dx, back_gate = (
        lax.all_to_all(
            summed_dx.astype(jnp.bfloat16), "ep", split_axis=0, concat_axis=0, tiled=True
        ).astype(summed_dx.dtype),
        lax.all_to_all(
            gate_sums.astype(jnp.bfloat16), "ep", split_axis=0, concat_axis=0, tiled=True
        ).astype(gate_sums.dtype),
    )
    slab_dx = jnp.sum(back_dx.reshape(experts, BLOCKS, capacity, col_width), axis=1)
    routed_dx = jnp.einsum("ect,ecd->td", per_token, slab_dx, precision=highest)
    slab_gate = jnp.sum(back_gate.reshape(experts, BLOCKS, capacity), axis=1)
    gate_grad = jnp.einsum("ecj,ec->j", assigned, slab_gate, precision=highest).reshape(
        tok_rows, top_count
    )
    logit_grad = logit_grads(picked, weights, gate_grad)
    router_cols = lax.dynamic_slice_in_dim(router, tp_index * col_width, col_width, 0).astype(
        jnp.float32
    )
    token_grad = (routed_dx + jnp.dot(logit_grad, router_cols.T, precision=highest)).astype(
        jnp.bfloat16
    )
    seg_rows = tok_rows // tp_count
    own_rows = lax.dynamic_slice_in_dim(tokens, tp_index * seg_rows, seg_rows, 0).astype(
        jnp.float32
    )
    own_logit = lax.dynamic_slice_in_dim(logit_grad, tp_index * seg_rows, seg_rows, 0)
    router_grad = lax.psum_scatter(
        jnp.dot(own_rows.T, own_logit, precision=highest),
        ("ep", "tp"),
        scatter_dimension=0,
        tiled=True,
    )
    return (token_grad, gate_grad, grad_gate[None], grad_up[None], grad_down[None], router_grad)


class Place:
    def __init__(self):
        self.line = lax.axis_size("ep") // BLOCKS
        ep, self.tp = lax.axis_index("ep"), lax.axis_index("tp")
        self.z, self.x = ep // BLOCKS, ep % BLOCKS
        self.y, self.c = self.tp // CORES, self.tp % CORES

    def ep(self, z, x):
        return z * BLOCKS + x

    def on_line(self, step):
        z = (self.z + step) % self.line
        return {"ep": self.ep(z, self.x), "tp": self.tp}

    def across(self):
        return {"ep": self.ep(self.z, 1 - self.x), "tp": self.tp}

    def other_plane(self):
        return {"ep": self.ep(self.z, self.x), "tp": (1 - self.y) * CORES + self.c}

    def other_core(self):
        return {"ep": self.ep(self.z, self.x), "tp": self.y * CORES + 1 - self.c}

    def greet(self):
        barrier = pltpu.get_barrier_semaphore()
        peers = [self.on_line(step) for step in range(1, self.line)]
        peers += [self.across(), self.other_plane(), self.other_core()]
        for peer in peers:
            pl.semaphore_signal(barrier, inc=1, device_id=peer, device_id_type=MESH)
        pl.semaphore_wait(barrier, len(peers))


def remote(src, dst, sems, index, peer):
    return pltpu.make_async_remote_copy(
        src_ref=src,
        dst_ref=dst,
        send_sem=sems.at[(0,) + index],
        recv_sem=sems.at[(1,) + index],
        device_id=peer,
        device_id_type=MESH,
    )


def gather_kernel(
    tok_ref, cot_ref, tok_out, cot_out, z_sems, x_sems, y_sems, c_sems, own_sems
):
    at = Place()
    line = at.line
    width = tok_ref.shape[1]
    half = width // CORES
    unit = half // 4
    ins, outs = (tok_ref, cot_ref), (tok_out, cot_out)
    own = at.ep(at.z, at.x)
    window = pl.ds(pl.multiple_of(at.c * half + at.y * unit, unit), half - unit)
    outer = pl.ds(pl.multiple_of(at.c * half + at.y * (half - unit), unit), unit)
    mine = pl.ds(pl.multiple_of(at.c * half, half), half)
    at.greet()

    started = []

    def send(src, dst, sems, index, peer):
        copy = remote(src, dst, sems, index, peer)
        copy.start()
        started.append(copy)

    for step in range(1, line):
        for i in range(2):
            send(
                ins[i].at[:, window], outs[i].at[own, :, window],
                z_sems, (step - 1, i), at.on_line(step),
            )
    for i in range(2):
        send(ins[i].at[:, window], outs[i].at[own, :, window], x_sems, (0, i), at.across())
    keep = [pltpu.make_async_copy(ins[i], outs[i].at[own], own_sems.at[i]) for i in range(2)]
    for copy in keep:
        copy.start()

    def arrived(sems, index, i, block, columns):
        ref = outs[i].at[block, :, columns]
        remote(ref, ref, sems, index, at.across()).wait_recv()

    def pass_on(block, columns, sems, index, peer, i):
        ref = outs[i].at[block, :, columns]
        send(ref, ref, sems, index, peer)

    blocks = []
    for step in range(1, line):
        block = at.ep((at.z - step + line) % line, at.x)
        blocks.append(block)
        for i in range(2):
            arrived(z_sems, (step - 1, i), i, block, window)
            pass_on(block, window, x_sems, (step, i), at.across(), i)
            pass_on(block, outer, y_sems, (step - 1, i), at.other_plane(), i)
    for step in range(line):
        block = at.ep((at.z - step + line) % line, 1 - at.x)
        blocks.append(block)
        for i in range(2):
            arrived(x_sems, (step, i), i, block, window)
            pass_on(block, outer, y_sems, (line - 1 + step, i), at.other_plane(), i)
    inner = pl.ds(pl.multiple_of(at.c * half + (1 - at.y) * (half - unit), unit), unit)
    for k, block in enumerate(blocks):
        for i in range(2):
            arrived(y_sems, (k, i), i, block, inner)
            pass_on(block, mine, c_sems, (k, i), at.other_core(), i)
    theirs = pl.ds(pl.multiple_of((1 - at.c) * half, half), half)
    for k, block in enumerate(blocks):
        for i in range(2):
            arrived(c_sems, (k, i), i, block, theirs)
    for copy in keep:
        copy.wait()
    for copy in started:
        copy.wait_send()


def gather_rows(tokens, cotangent):
    ep_count = lax.axis_size("ep")
    line = ep_count // BLOCKS
    rows, width = tokens.shape
    whole = jax.ShapeDtypeStruct((ep_count, rows, width), tokens.dtype)
    dma = pltpu.SemaphoreType.DMA
    tok_all, cot_all = pl.pallas_call(
        gather_kernel,
        out_shape=(whole, whole),
        in_specs=[pl.BlockSpec(memory_space=pltpu.VMEM)] * 2,
        out_specs=[pl.BlockSpec(memory_space=pltpu.VMEM)] * 2,
        scratch_shapes=[
            dma((2, line - 1, 2)),
            dma((2, line, 2)),
            dma((2, ep_count - 1, 2)),
            dma((2, ep_count - 1, 2)),
            dma((2,)),
        ],
        compiler_params=pltpu.CompilerParams(collective_id=0, has_side_effects=True),
    )(tokens, cotangent)
    return tok_all.reshape(-1, width), cot_all.reshape(-1, width)


def scatter_kernel(
    dx_ref, gate_ref, out_ref, gate_out, c_recv, y_send, y_recv, x_send, x_recv, z_send, z_recv, total,
    g_send, g_recv, c_sems, y_sems, x_sems, z_sems, g_sems,
):
    at = Place()
    line = at.line
    part = out_ref.shape[1]

    def columns(plane, core):
        return pl.ds(pl.multiple_of((plane * CORES + core) * part, part), part)

    def f32(value):
        return value.astype(jnp.float32)

    at.greet()
    started = []

    def send(src, dst, sems, index, peer):
        copy = remote(src, dst, sems, index, peer)
        copy.start()
        started.append(copy)

    def arrived(ref, sems, index):
        remote(ref, ref, sems, index, at.across()).wait_recv()

    blocks = [
        at.ep((at.z + 1 + j) % line, x) for x in (1 - at.x, at.x) for j in range(line)
    ]
    for k, block in enumerate(blocks):
        for p in range(2):
            send(
                dx_ref.at[block, :, columns(p, 1 - at.c)], c_recv.at[k, p],
                c_sems, (k, p), at.other_core(),
            )
    gate_out[...] = gate_ref[...]
    stages = (at.other_core(), at.other_plane(), at.across())
    for n, peer in enumerate(stages):
        g_send[n] = gate_out[...]
        send(g_send.at[n], g_recv.at[n], g_sems, (n,), peer)
        arrived(g_recv.at[n], g_sems, (n,))
        gate_out[...] += g_recv[n]
    last = len(stages)
    g_send[last] = gate_out[...]
    for step in range(1, line):
        n = last + step - 1
        send(g_send.at[last], g_recv.at[n], g_sems, (n,), at.on_line(step))
    for k, block in enumerate(blocks):
        for p in range(2):
            arrived(c_recv.at[k, p], c_sems, (k, p))
        y_send[k] = (
            f32(dx_ref[block, :, columns(1 - at.y, at.c)]) + f32(c_recv[k, 1 - at.y])
        ).astype(y_send.dtype)
        send(y_send.at[k], y_recv.at[k], y_sems, (k,), at.other_plane())
        total[k] = f32(dx_ref[block, :, columns(at.y, at.c)]) + f32(c_recv[k, at.y])
    for j in range(line):
        arrived(y_recv.at[j], y_sems, (j,))
        x_send[j] = (total[j] + f32(y_recv[j])).astype(x_send.dtype)
        send(x_send.at[j], x_recv.at[j], x_sems, (j,), at.across())
    for j in range(line):
        k = line + j
        arrived(y_recv.at[k], y_sems, (k,))
        arrived(x_recv.at[j], x_sems, (j,))
        summed = total[k] + f32(y_recv[k]) + f32(x_recv[j])
        if j < line - 1:
            z_send[j] = summed.astype(z_send.dtype)
            send(z_send.at[j], z_recv.at[j], z_sems, (j,), at.on_line(1 + j))
        else:
            out_ref[...] = summed
    for j in range(line - 1):
        arrived(z_recv.at[j], z_sems, (j,))
        out_ref[...] += f32(z_recv[j])
    for n in range(last, last + line - 1):
        arrived(g_recv.at[n], g_sems, (n,))
        gate_out[...] += g_recv[n]
    for copy in started:
        copy.wait_send()


def scatter_rows(partial, gates):
    ep_count, tp_count = lax.axis_size("ep"), lax.axis_size("tp")
    line = ep_count // BLOCKS
    width = partial.shape[1]
    rows, part = partial.shape[0] // ep_count, width // tp_count
    dma = pltpu.SemaphoreType.DMA

    def slots(*lead, kind=partial.dtype):
        return pltpu.VMEM(lead + (rows, part), kind)

    return pl.pallas_call(
        scatter_kernel,
        out_shape=(
            jax.ShapeDtypeStruct((rows, part), jnp.float32),
            jax.ShapeDtypeStruct(gates.shape, gates.dtype),
        ),
        in_specs=[pl.BlockSpec(memory_space=pltpu.VMEM)] * 2,
        out_specs=[pl.BlockSpec(memory_space=pltpu.VMEM)] * 2,
        scratch_shapes=[
            slots(ep_count, 2),
            slots(ep_count),
            slots(ep_count),
            slots(line),
            slots(line),
            slots(line - 1),
            slots(line - 1),
            slots(ep_count, kind=jnp.float32),
            pltpu.VMEM((4,) + gates.shape, gates.dtype),
            pltpu.VMEM((2 + line,) + gates.shape, gates.dtype),
            dma((2, ep_count, 2)),
            dma((2, ep_count)),
            dma((2, line)),
            dma((2, line - 1)),
            dma((2, 2 + line)),
        ],
        compiler_params=pltpu.CompilerParams(collective_id=1, has_side_effects=True),
    )(partial.reshape(ep_count, rows, width), gates)


def dense_shards(tokens, cotangent, routes, router, w_gate, w_up, w_down):
    highest = lax.Precision.HIGHEST
    ep_count = lax.axis_size("ep")
    tp_count = lax.axis_size("tp")
    experts = ep_count // BLOCKS
    tok_rows, width = tokens.shape
    col_width = width // tp_count
    ep_index = lax.axis_index("ep")
    tp_index = lax.axis_index("tp")
    expert = ep_index // BLOCKS
    w_gate, w_up, w_down = w_gate[0], w_up[0], w_down[0]

    routes_t = lax.all_gather(routes.T.astype(jnp.float32), "ep", axis=1, tiled=True)
    routes_t = routes_t.astype(jnp.int32)
    tok_all, cot_all = gather_rows(tokens, cotangent)

    logits = lax.dot_general(
        router, tok_all, (((0,), (1,)), ((), ())), preferred_element_type=jnp.float32
    )
    labels = jnp.arange(experts, dtype=jnp.int32)[:, None]
    picked = [(routes_t[k][None, :] == labels).astype(jnp.float32) for k in range(2)]
    chosen = [jnp.sum(p * logits, axis=0) for p in picked]
    margin = chosen[0] - chosen[1]
    weights = [jax.nn.sigmoid(margin), jax.nn.sigmoid(-margin)]
    sent = [w.astype(jnp.bfloat16).astype(jnp.float32) for w in weights]
    mine = [(routes_t[k] == expert).astype(jnp.float32) for k in range(2)]
    gate_col = (mine[0] * sent[0] + mine[1] * sent[1])[:, None]

    pre_gate = jnp.dot(tok_all, w_gate, preferred_element_type=jnp.float32)
    pre_up = jnp.dot(tok_all, w_up, preferred_element_type=jnp.float32)
    back_grad = lax.dot_general(
        cot_all, w_down, (((1,), (1,)), ((), ())), preferred_element_type=jnp.float32
    )
    sig_gate = jax.nn.sigmoid(pre_gate)
    active = pre_gate * sig_gate
    hidden = (active * pre_up).astype(jnp.bfloat16)
    gate_terms = jnp.sum(hidden.astype(jnp.float32) * back_grad, axis=1)
    scaled_back = gate_col * back_grad
    d_gate = (scaled_back * pre_up * sig_gate * (1.0 + pre_gate * (1.0 - sig_gate))).astype(
        jnp.bfloat16
    )
    d_up = (scaled_back * active).astype(jnp.bfloat16)
    scaled_cot = (gate_col * cot_all.astype(jnp.float32)).astype(jnp.bfloat16)

    contract_hidden = (((1,), (1,)), ((), ()))
    partial_dx = lax.dot_general(
        d_gate, w_gate, contract_hidden, preferred_element_type=jnp.float32
    )
    partial_dx = partial_dx + lax.dot_general(
        d_up, w_up, contract_hidden, preferred_element_type=jnp.float32
    )
    routed_dx, gate_sum = scatter_rows(
        partial_dx.astype(jnp.bfloat16),
        jnp.stack([mine[0] * gate_terms, mine[1] * gate_terms]),
    )

    contract_rows = (((0,), (0,)), ((), ()))
    grad_gate = lax.dot_general(
        tok_all, d_gate, contract_rows, preferred_element_type=jnp.float32
    ).astype(jnp.bfloat16)
    grad_up = lax.dot_general(
        tok_all, d_up, contract_rows, preferred_element_type=jnp.float32
    ).astype(jnp.bfloat16)
    grad_down = lax.dot_general(
        hidden, scaled_cot, contract_rows, preferred_element_type=jnp.float32
    ).astype(jnp.bfloat16)

    lead = weights[0] * weights[1] * (gate_sum[0] - gate_sum[1])
    logit_grad = (picked[0] - picked[1]) * lead[None, :]
    own_logit = lax.dynamic_slice_in_dim(logit_grad, ep_index * tok_rows, tok_rows, 1)
    gate_grad = lax.dynamic_slice_in_dim(gate_sum, ep_index * tok_rows, tok_rows, 1).T
    router_cols = lax.dynamic_slice_in_dim(router, tp_index * col_width, col_width, 0)
    token_grad = (
        routed_dx
        + lax.dot_general(
            own_logit,
            router_cols.astype(jnp.float32),
            (((0,), (1,)), ((), ())),
            precision=highest,
        )
    ).astype(jnp.bfloat16)
    seg = width // (ep_count * tp_count)
    own_cols = lax.dynamic_slice_in_dim(
        tok_all, (ep_index * tp_count + tp_index) * seg, seg, 1
    ).astype(jnp.float32)
    router_grad = lax.dot_general(
        logit_grad, own_cols, (((1,), (0,)), ((), ())), precision=highest
    ).T
    return (token_grad, gate_grad, grad_gate[None], grad_up[None], grad_down[None], router_grad)


def shards(tokens, cotangent, routes, router, w_gate, w_up, w_down):
    slots = 3 * routes.shape[1] * BLOCKS
    dense = slots >= lax.axis_size("ep") and lax.axis_size("tp") == 2 * CORES
    path = dense_shards if dense else routed_shards
    return path(tokens, cotangent, routes, router, w_gate, w_up, w_down)


def solution(mesh):
    placed = (
        P("ep", None),
        P("ep", None),
        P("ep", None),
        P(),
        P("ep", None, "tp"),
        P("ep", None, "tp"),
        P("ep", "tp", None),
    )
    return jax.shard_map(
        shards,
        mesh=mesh,
        in_specs=placed,
        out_specs=(
            P("ep", "tp"),
            P("ep", None),
            P("ep", None, "tp"),
            P("ep", None, "tp"),
            P("ep", "tp", None),
            P(("ep", "tp"), None),
        ),
        check_vma=False,
    )
```

profile of v0, /device:TPU:0, one launch (start us, length us, event | category | flops | bytes accessed | tf_op | source)
XLA Modules:
  0.0 160.5 jit_solution(198280228548388245)
XLA Ops:
  0.6 0.0 copy-start
  0.7 0.8 convert_bitcast_fusion
  1.5 22.4 %all_gather.3 = f32[2,1024]{1,0:T(2,128)S(1)} all-gather(f32[2,128]{1,0:T(2,128)S(1)} %convert_bitcast_fusion), channel_id=1, replica_groups=mesh['ep'=8,'tp'=4] {'ep'}, dimensions={1}, use_global_device_ids=true | all-gather | bytes 9216 | tf_op jit(solution)/shard_map/all_gather | solution.py:432
  23.9 48.4 %shard_map.118 = (bf16[8,128,2048]{2,1,0:T(8,128)(2,1)}, bf16[8,128,2048]{2,1,0:T(8,128)(2,1)}) custom-call(bf16[128,2048]{1,0:T(8,128)(2,1)} %tok_ref.1, bf16[128,2048]{1,0:T(8,128)(2,1)} %cot_ref.1), custom_call_target="tpu_custom_call" | custom-call | tf_op jit(solution)/shard_map/pallas_call | solution.py:286
  72.3 0.0 copy-start.1
  72.3 3.5 %select_reduce_fusion = (f32[1024]{0:T(1024)S(1)}, f32[1024]{0:T(1024)S(1)}) fusion(s32[1024]{0:T(1024)S(1)} %bitcast.58, s32[1024]{0:T(1024)S(1)} %bitcast.54, bf16[1024,2048]{1,0:T(8,128)(2,1)} %bitcast.47, bf16[2048,4]{0,1:T(4,128)(2,1)} %param.10), kind=kOutput, calls=%fused_computation.31 | convolution fusion | flops 16799744 | bytes 4227072 | tf_op jit(solution)/shard_map/dot_general | solution.py:436
  75.9 0.0 copy-done
  75.9 0.0 copy-done.1
  75.9 0.0 copy-start.4
  75.9 2.4 %fusion.8 = f32[1024,512]{0,1:T(8,128)S(1)} fusion(bf16[1024,2048]{1,0:T(8,128)(2,1)S(1)} %bitcast.49, bf16[1,2048,512]{2,1,0:T(8,128)(2,1)S(1)} %copy-done), kind=kOutput, calls=%fused_computation.12 | convolution fusion | flops 2147483648 | bytes 8388608 | tf_op jit(solution)/shard_map/dot_general | solution.py:448
  78.4 0.0 copy-done.4
  78.4 0.0 copy-start.2
  78.4 0.0 copy-start.3
  78.4 2.4 %fusion.11 = f32[1024,512]{0,1:T(8,128)S(1)} fusion(bf16[1024,2048]{1,0:T(8,128)(2,1)S(1)} %bitcast.50, bf16[1,2048,512]{2,1,0:T(8,128)(2,1)S(1)} %copy-done.4), kind=kOutput, calls=%fused_computation.15 | convolution fusion | flops 2147483648 | bytes 8388608 | tf_op jit(solution)/shard_map/dot_general | solution.py:449
  80.8 0.0 copy-done.2
  80.8 0.4 copy-done.3
  81.2 3.2 %multiply_reduce_fusion = (f32[1024]{0:T(1024)S(1)}, bf16[1024,512]{0,1:T(8,128)(2,1)S(1)}, bf16[1024,512]{0,1:T(8,128)(2,1)S(1)}, bf16[1024,512]{0,1:T(8,128)(2,1)S(1)}) fusion(f32[1024,512]{0,1:T(8,128)S(1)} %fusion.11, f32[1024,512]{0,1:T(8,128)S(1)} %fusion.8, f32[1024]{0:T(1024)S(1)} %get-tuple-element.23, bf16[1024,2048]{1,0:T(8,128)(2,1)S(1)} %bitcast.66, ...), kind=kOutput, calls=%fused_computation.19 | convolution fusion | flops 2157444096 | bytes 13639680 | tf_op jit(solution)/shard_map/dot_general | solution.py:450
  84.5 3.8 %fusion.3 = bf16[1,512,2048]{2,1,0:T(8,128)(2,1)} fusion(bf16[1024,512]{0,1:T(8,128)(2,1)S(1)} %get-tuple-element.17, bf16[1024,2048]{1,0:T(8,128)(2,1)S(1)} %bitcast.67, f32[1024]{0:T(1024)S(1)} %get-tuple-element.23), kind=kOutput, calls=%fused_computation.7 | convolution fusion | flops 2154823680 | bytes 7344128 | tf_op jit(solution)/shard_map/dot_general | solution.py:483
  88.3 0.6 pad_maximum_fusion.gate_ref
  88.9 4.0 %fusion.4 = bf16[1,2048,512]{2,1,0:T(8,128)(2,1)} fusion(bf16[1024,2048]{1,0:T(8,128)(2,1)S(1)} %bitcast.51, bf16[1024,512]{0,1:T(8,128)(2,1)S(1)} %get-tuple-element.18), kind=kOutput, calls=%fused_computation.8 | convolution fusion | flops 2148532224 | bytes 7340032 | tf_op jit(solution)/shard_map/dot_general | solution.py:477
  92.9 3.8 %fusion.5 = bf16[1,2048,512]{2,1,0:T(8,128)(2,1)} fusion(bf16[1024,2048]{1,0:T(8,128)(2,1)S(1)} %bitcast.52, bf16[1024,512]{0,1:T(8,128)(2,1)S(1)} %get-tuple-element.19), kind=kOutput, calls=%fused_computation.9 | convolution fusion | flops 2148532224 | bytes 7340032 | tf_op jit(solution)/shard_map/dot_general | solution.py:480
  96.7 2.4 %fusion.6 = f32[1024,2048]{1,0:T(8,128)S(1)} fusion(bf16[1024,512]{0,1:T(8,128)(2,1)S(1)} %get-tuple-element.18, bf16[1,2048,512]{2,1,0:T(8,128)(2,1)S(1)} %copy-done), kind=kOutput, calls=%fused_computation.10 | convolution fusion | flops 2147483648 | bytes 11534336 | tf_op jit(solution)/shard_map/dot_general | solution.py:465
  99.1 4.4 %add_convert_fusion = bf16[1024,2048]{1,0:T(8,128)(2,1)} fusion(f32[1024,2048]{1,0:T(8,128)S(1)} %fusion.6, bf16[1024,512]{0,1:T(8,128)(2,1)S(1)} %get-tuple-element.19, bf16[1,2048,512]{2,1,0:T(8,128)(2,1)S(1)} %copy-done.4), kind=kOutput, calls=%fused_computation.1 | convolution fusion | flops 2151677952 | bytes 15728640 | tf_op jit(solution)/shard_map/dot_general | solution.py:468
  103.5 51.2 %shard_map.119 = (f32[128,512]{1,0:T(8,128)}, f32[2,1024]{1,0:T(2,128)}) custom-call(bf16[8,128,2048]{2,1,0:T(8,128)(2,1)} %bitcast.53, f32[2,1024]{1,0:T(2,128)} %pad_maximum_fusion.gate_ref), custom_call_target="tpu_custom_call" | custom-call | tf_op jit(solution)/shard_map/pallas_call | solution.py:391
  154.7 0.8 subtract_multiply_fusion.1
  155.5 1.2 dynamic-slice_bitcast_fusion
  156.7 1.9 %fusion.17 = f32[64,4]{0,1:T(4,128)} fusion(bf16[1024,2048]{1,0:T(8,128)(2,1)} %bitcast.48, s32[]{:T(128)S(6)} %select_n.18, f32[1024]{0:T(1024)S(1)} %bitcast.62, s32[1024]{0:T(1024)S(1)} %bitcast.60, s32[1024]{0:T(1024)S(1)} %bitcast.56), kind=kOutput, calls=%fused_computation.28 | convolution fusion | flops 3170304 | bytes 275460 | tf_op jit(solution)/shard_map/dot_general | solution.py:505
  158.6 2.0 %fusion.16 = bf16[128,512]{1,0:T(8,128)(2,1)} fusion(f32[128,512]{1,0:T(8,128)} %get-tuple-element.12, bf16[2048,4]{0,1:T(4,128)(2,1)} %param.10, s32[]{:T(128)S(6)} %select_n.17, f32[4,1024]{1,0:T(4,128)S(1)} %subtract_multiply_fusion, s32[]{:T(128)S(6)} %select_n.16), kind=kOutput, calls=%fused_computation.26 | convolution fusion | flops 3276800 | bytes 399368 | tf_op jit(solution)/shard_map/dot_general | solution.py:494
  (5 shorter events, 0.1 us)
Async XLA Ops:
  0.6 75.3 %copy-start = (bf16[1,2048,512]{2,1,0:T(8,128)(2,1)S(1)}, bf16[1,2048,512]{2,1,0:T(8,128)(2,1)}, u32[]{:S(2)}) copy-start(bf16[1,2048,512]{2,1,0:T(8,128)(2,1)} %param.11) | copy-start | bytes 6291460
  72.3 3.6 %copy-start.1 = (bf16[8,128,2048]{2,1,0:T(8,128)(2,1)S(1)}, bf16[8,128,2048]{2,1,0:T(8,128)(2,1)}, u32[]{:S(2)}) copy-start(bf16[8,128,2048]{2,1,0:T(8,128)(2,1)} %get-tuple-element.10) | copy-start | bytes 12582916
  75.9 2.4 %copy-start.4 = (bf16[1,2048,512]{2,1,0:T(8,128)(2,1)S(1)}, bf16[1,2048,512]{2,1,0:T(8,128)(2,1)}, u32[]{:S(2)}) copy-start(bf16[1,2048,512]{2,1,0:T(8,128)(2,1)} %param.12) | copy-start | bytes 6291460
  78.4 2.5 %copy-start.2 = (bf16[8,128,2048]{2,1,0:T(8,128)(2,1)S(1)}, bf16[8,128,2048]{2,1,0:T(8,128)(2,1)}, u32[]{:S(2)}) copy-start(bf16[8,128,2048]{2,1,0:T(8,128)(2,1)} %get-tuple-element.11) | copy-start | bytes 12582916
  78.4 2.9 %copy-start.3 = (bf16[1,512,2048]{2,1,0:T(8,128)(2,1)S(1)}, bf16[1,512,2048]{2,1,0:T(8,128)(2,1)}, u32[]{:S(2)}) copy-start(bf16[1,512,2048]{2,1,0:T(8,128)(2,1)} %param.13) | copy-start | bytes 6291460
where the time goes:
time: 161 us
  Pallas kernels  99.6 us (62%)
  matrix products  33.8 us (21%)
  blocking collectives  22.4 us (14%)
  other arithmetic  2.26 us (1%)
  local copies, waits for them, and re-layouts  1.69 us (1%)
    pallas_call x1, Pallas kernels, scatter_rows(): pl.pallas_call(scatter_kernel, out_shape=(jax.ShapeDtypeStruct((rows, par...  51.2 us
    pallas_call x1, Pallas kernels, gather_rows(): pl.pallas_call(gather_kernel, out_shape=(whole, whole), in_specs=[pl.Bloc...  48.4 us
    all_gather x1, blocking collectives, dense_shards(): lax.all_gather(routes.T.astype(jnp.float32), 'ep', axis=1, tiled=True)  22.4 us
    dot_general x1, matrix products, dense_shards(): lax.dot_general(d_up, w_up, contract_hidden, preferred_element_type=jnp.f...  4.36 us
    dot_general x1, matrix products, dense_shards(): lax.dot_general(tok_all, d_gate, contract_rows, preferred_element_type=jn...  4.04 us
    dot_general x1, matrix products, dense_shards(): lax.dot_general(tok_all, d_up, contract_rows, preferred_element_type=jnp....  3.82 us
    dot_general x1, matrix products, dense_shards(): lax.dot_general(hidden, scaled_cot, contract_rows, preferred_element_type...  3.77 us
    dot_general x1, matrix products, dense_shards(): lax.dot_general(router, tok_all, (((0,), (1,)), ((), ())), preferred_elem...  3.54 us

commit v1 on v0

v1 whole, which is shorter than its diff:
```python
import jax
import jax.numpy as jnp
from jax import lax
from jax.experimental import pallas as pl
from jax.experimental.pallas import tpu as pltpu
from jax.sharding import PartitionSpec as P

BLOCKS = 2
CORES = 2
PLANES = 2
LINE = 4
PIECES = 2
MESH = pl.DeviceIdType.MESH


def build_slots(block_routes, experts, capacity):
    flat_routes = block_routes.reshape(-1)
    labels = jnp.arange(experts, dtype=jnp.int32)
    hit_mask = (flat_routes[None, :] == labels[:, None]).astype(jnp.int32)
    rank_in = jnp.cumsum(hit_mask, axis=1, dtype=jnp.int32) - 1
    slot_ids = jnp.arange(capacity, dtype=jnp.int32)
    assigned = (hit_mask[:, None, :] == 1) & (rank_in[:, None, :] == slot_ids[None, :, None])
    return assigned.astype(jnp.float32)


def gate_pair(tokens, routes, router, experts):
    logits = jnp.dot(tokens, router, preferred_element_type=jnp.float32)
    labels = jnp.arange(experts, dtype=jnp.int32)
    picked = (routes[:, :, None] == labels[None, None, :]).astype(jnp.float32)
    chosen = jnp.sum(picked * logits[:, None, :], axis=2)
    margin = chosen[:, 0] - chosen[:, 1]
    weights = jnp.stack([jax.nn.sigmoid(margin), jax.nn.sigmoid(-margin)], axis=1)
    return (picked, weights)


def logit_grads(picked, weights, gate_grad):
    lead_grad = weights[:, 0] * weights[:, 1] * (gate_grad[:, 0] - gate_grad[:, 1])
    pair_grad = jnp.stack([lead_grad, -lead_grad], axis=1)
    return jnp.sum(picked * pair_grad[:, :, None], axis=1)


def expert_grads(rows_in, cot_in, gate_in, gate_weight, up_weight, down_weight):
    pre_gate = jnp.dot(rows_in, gate_weight, preferred_element_type=jnp.float32)
    pre_up = jnp.dot(rows_in, up_weight, preferred_element_type=jnp.float32)
    back_grad = lax.dot_general(
        cot_in, down_weight, (((1,), (1,)), ((), ())), preferred_element_type=jnp.float32
    )
    sig_gate = jax.nn.sigmoid(pre_gate)
    active = pre_gate * sig_gate
    hidden = (active * pre_up).astype(jnp.bfloat16)
    gate_terms = jnp.sum(hidden.astype(jnp.float32) * back_grad, axis=1)
    gate_col = gate_in.astype(jnp.float32)[:, None]
    scaled_back = gate_col * back_grad
    d_gate = (scaled_back * pre_up * sig_gate * (1.0 + pre_gate * (1.0 - sig_gate))).astype(
        jnp.bfloat16
    )
    d_up = (scaled_back * active).astype(jnp.bfloat16)
    scaled_cot = (gate_col * cot_in.astype(jnp.float32)).astype(jnp.bfloat16)
    contract_rows = (((0,), (0,)), ((), ()))
    grad_gate = lax.dot_general(
        rows_in, d_gate, contract_rows, preferred_element_type=jnp.float32
    ).astype(jnp.bfloat16)
    grad_up = lax.dot_general(
        rows_in, d_up, contract_rows, preferred_element_type=jnp.float32
    ).astype(jnp.bfloat16)
    grad_down = lax.dot_general(
        hidden, scaled_cot, contract_rows, preferred_element_type=jnp.float32
    ).astype(jnp.bfloat16)
    return (d_gate, d_up, gate_terms, grad_gate, grad_up, grad_down)


def spread_slabs(packed, experts, slab_count):
    widened = jnp.broadcast_to(packed[:, None], (experts, BLOCKS) + packed.shape[1:])
    return widened.reshape((slab_count,) + packed.shape[1:])


def routed_shards(tokens, cotangent, routes, router, w_gate, w_up, w_down):
    highest = lax.Precision.HIGHEST
    ep_count = lax.axis_size("ep")
    tp_count = lax.axis_size("tp")
    experts = ep_count // BLOCKS
    tok_rows, width = tokens.shape
    top_count = routes.shape[1]
    capacity = 3 * tok_rows * top_count // (2 * experts)
    col_width = width // tp_count
    tp_index = lax.axis_index("tp")
    picked, weights = gate_pair(tokens, routes, router, experts)
    assigned = build_slots(routes, experts, capacity)
    per_token = jnp.sum(assigned.reshape(experts, capacity, tok_rows, top_count), axis=3)
    token_map = per_token.astype(jnp.bfloat16)
    gate_send = weights.astype(jnp.bfloat16)
    gate_slots = jnp.einsum(
        "ecj,j->ec", assigned, gate_send.astype(jnp.float32).reshape(-1), precision=highest
    ).astype(jnp.bfloat16)
    gate_out = spread_slabs(gate_slots, experts, ep_count)

    def pack_rows(source):
        packed = jnp.einsum(
            "ect,td->ecd", token_map, source, preferred_element_type=jnp.float32
        ).astype(jnp.bfloat16)
        return spread_slabs(packed, experts, ep_count)

    tok_part = lax.dynamic_slice_in_dim(tokens, tp_index * col_width, col_width, 1)
    cot_part = lax.dynamic_slice_in_dim(cotangent, tp_index * col_width, col_width, 1)
    recv_part, recv_cot_part, recv_gate = (
        lax.all_to_all(pack_rows(tok_part), "ep", split_axis=0, concat_axis=0, tiled=True),
        lax.all_to_all(pack_rows(cot_part), "ep", split_axis=0, concat_axis=0, tiled=True),
        lax.all_to_all(gate_out, "ep", split_axis=0, concat_axis=0, tiled=True),
    )
    recv_rows, recv_cot = (
        lax.all_gather(recv_part, "tp", axis=2, tiled=True),
        lax.all_gather(recv_cot_part, "tp", axis=2, tiled=True),
    )
    rows_in = recv_rows.reshape(-1, width)
    cot_in = recv_cot.reshape(-1, width)
    gate_in = recv_gate.reshape(-1)
    d_gate, d_up, gate_terms, grad_gate, grad_up, grad_down = expert_grads(
        rows_in, cot_in, gate_in, w_gate[0], w_up[0], w_down[0]
    )
    contract_hidden = (((1,), (1,)), ((), ()))
    partial_dx = lax.dot_general(
        d_gate, w_gate[0], contract_hidden, preferred_element_type=jnp.float32
    )
    partial_dx = partial_dx + lax.dot_general(
        d_up, w_up[0], contract_hidden, preferred_element_type=jnp.float32
    )
    summed_dx = lax.psum_scatter(
        partial_dx.reshape(ep_count, capacity, width).astype(jnp.bfloat16),
        "tp",
        scatter_dimension=2,
        tiled=True,
    ).astype(jnp.float32)
    gate_sums = lax.psum(gate_terms.reshape(ep_count, capacity), "tp")
    back_dx, back_gate = (
        lax.all_to_all(
            summed_dx.astype(jnp.bfloat16), "ep", split_axis=0, concat_axis=0, tiled=True
        ).astype(summed_dx.dtype),
        lax.all_to_all(
            gate_sums.astype(jnp.bfloat16), "ep", split_axis=0, concat_axis=0, tiled=True
        ).astype(gate_sums.dtype),
    )
    slab_dx = jnp.sum(back_dx.reshape(experts, BLOCKS, capacity, col_width), axis=1)
    routed_dx = jnp.einsum("ect,ecd->td", per_token, slab_dx, precision=highest)
    slab_gate = jnp.sum(back_gate.reshape(experts, BLOCKS, capacity), axis=1)
    gate_grad = jnp.einsum("ecj,ec->j", assigned, slab_gate, precision=highest).reshape(
        tok_rows, top_count
    )
    logit_grad = logit_grads(picked, weights, gate_grad)
    router_cols = lax.dynamic_slice_in_dim(router, tp_index * col_width, col_width, 0).astype(
        jnp.float32
    )
    token_grad = (routed_dx + jnp.dot(logit_grad, router_cols.T, precision=highest)).astype(
        jnp.bfloat16
    )
    seg_rows = tok_rows // tp_count
    own_rows = lax.dynamic_slice_in_dim(tokens, tp_index * seg_rows, seg_rows, 0).astype(
        jnp.float32
    )
    own_logit = lax.dynamic_slice_in_dim(logit_grad, tp_index * seg_rows, seg_rows, 0)
    router_grad = lax.psum_scatter(
        jnp.dot(own_rows.T, own_logit, precision=highest),
        ("ep", "tp"),
        scatter_dimension=0,
        tiled=True,
    )
    return (token_grad, gate_grad, grad_gate[None], grad_up[None], grad_down[None], router_grad)


class Place:
    def __init__(self):
        ep, self.tp = lax.axis_index("ep"), lax.axis_index("tp")
        self.z, self.x = ep // BLOCKS, ep % BLOCKS
        self.y, self.c = self.tp // CORES, self.tp % CORES
        self.pair = self.z + 1 - 2 * (self.z % 2)
        self.near = 2 - self.z // 2
        self.far = 3 * (1 - self.z // 2)
        self.rank = 3 - (self.z + 1) // 2 % 2
        self.lines = (self.pair, self.near, self.far)
        self.slots = (1, self.rank, self.rank)

    def device(self, z, x):
        return {"ep": z * BLOCKS + x, "tp": self.tp}

    def along(self, z):
        return self.device(z, self.x)

    def across(self):
        return self.device(self.z, 1 - self.x)

    def other_plane(self):
        return {"ep": self.z * BLOCKS + self.x, "tp": (1 - self.y) * CORES + self.c}

    def other_core(self):
        return {"ep": self.z * BLOCKS + self.x, "tp": self.y * CORES + 1 - self.c}

    def turned(self, step, flip):
        return self.device((self.z + step) % LINE, (self.x + flip) % BLOCKS)

    def greet(self):
        barrier = pltpu.get_barrier_semaphore()
        peers = [self.turned(step, flip) for step in range(LINE) for flip in range(2)][1:]
        peers += [self.other_plane(), self.other_core()]
        for peer in peers:
            pl.semaphore_signal(barrier, inc=1, device_id=peer, device_id_type=MESH)
        pl.semaphore_wait(barrier, len(peers))


SCHEDULE = (
    "X0", "Z1", "Y01", "Y10", "F0", "X1", "Z2", "Y11", "D0", "Y20", "A0", "F1", "X2", "Z3",
    "B0", "D1", "Y21", "Y30", "E0", "A1", "X3", "F2", "B1", "D2", "Y31", "E1", "A2", "F3", "G0",
    "D3", "G1", "B2", "A3", "G2", "E2", "W0", "B3", "G3", "W1", "E3", "W2", "G4", "T", "R",
)


def fused_kernel(
    tok_hbm, cot_hbm, routes_ref, router_ref, wg_hbm, wu_hbm, wd_hbm,
    tg_ref, gg_ref, gw_ref, gu_ref, gd_ref, rg_ref,
    src, wgu, wd, rows, pack, hot, gate_send, gate_recv, gate_col,
    hs, dgu, dx_send, dx_own, c_recv, y_send, y_recv, y_own, x_send, x_recv, z_send, z_recv,
    g_sum, g_send, g_recv, gz_recv, r_send, r_recv,
    load_sems, z_sems, x_sems, y_sems, c_sems, gz_sems, gx_sems,
    sc_sems, sy_sems, sx_sems, sz_sems, gp_sems, gl_sems, r_sems,
):
    f32, bf16 = jnp.float32, jnp.bfloat16
    at = Place()
    cap, tok_rows, width = pack.shape[1], src.shape[1], src.shape[2]
    hidden, part = wd.shape[0], tg_ref.shape[1]
    span = pack.shape[2]
    rest = width - span
    size = cap // PIECES
    window = pl.ds(pl.multiple_of(at.y * rest, 128), span)
    outer = pl.ds(pl.multiple_of(at.y * span, 128), rest)
    inner = pl.ds(pl.multiple_of((1 - at.y) * span, 128), rest)
    started = []

    def dot(lhs, rhs, dims):
        return lax.dot_general(lhs, rhs, (dims, ((), ())), preferred_element_type=f32)

    def send(source, target, send_sem, recv_sem, peer):
        copy = pltpu.make_async_remote_copy(
            src_ref=source, dst_ref=target, send_sem=send_sem, recv_sem=recv_sem,
            device_id=peer, device_id_type=MESH,
        )
        copy.start()
        started.append(copy)

    def arrived(target, sem):
        pltpu.make_async_remote_copy(
            src_ref=target, dst_ref=target, send_sem=sem, recv_sem=sem,
            device_id=at.across(), device_id_type=MESH,
        ).wait_recv()

    loads = [
        pltpu.make_async_copy(tok_hbm, src.at[0], load_sems.at[0]),
        pltpu.make_async_copy(cot_hbm, src.at[1], load_sems.at[1]),
        pltpu.make_async_copy(wg_hbm, wgu.at[:, pl.ds(0, hidden)], load_sems.at[2]),
        pltpu.make_async_copy(wu_hbm, wgu.at[:, pl.ds(hidden, hidden)], load_sems.at[3]),
        pltpu.make_async_copy(wd_hbm, wd, load_sems.at[4]),
    ]
    for copy in loads:
        copy.start()

    side = hot.shape[1]
    row8 = lax.broadcasted_iota(jnp.int32, (8, tok_rows), 0)
    first, second = routes_ref[0:1, :], routes_ref[1:2, :]
    is_first, is_second = first == row8, second == row8
    hit = jnp.where(is_first | is_second, 1.0, 0.0)
    up_to = lax.broadcasted_iota(jnp.int32, (tok_rows, tok_rows), 0) <= lax.broadcasted_iota(
        jnp.int32, (tok_rows, tok_rows), 1
    )
    place = dot(hit, jnp.where(up_to, 1.0, 0.0), ((1,), (0,)))
    place = jnp.where(hit > 0.0, place, 0.0)
    slot = (lax.broadcasted_iota(jnp.int32, (side, tok_rows), 0) + 1).astype(f32)
    for e in range(LINE):
        hot[e] = jnp.where(slot == place[e : e + 1, :], 1.0, 0.0).astype(bf16)
    at.greet()

    loads[0].wait()
    loads[1].wait()

    def piece(k, j, h):
        return pl.ds((k * BLOCKS + j) * cap + h * size, size)

    def chunk(k):
        return slice(k * BLOCKS * cap, (k + 1) * BLOCKS * cap)

    def pass_x(k, h):
        send(
            rows.at[at.c, piece(k, 0, h), window], rows.at[at.c, piece(k, 1, h), window],
            x_sems.at[0, k, h], x_sems.at[1, k, h], at.across(),
        )

    def pass_y(k, j, h):
        ref = rows.at[at.c, piece(k, j, h), outer]
        send(ref, ref, y_sems.at[0, k, j, h], y_sems.at[1, k, j, h], at.other_plane())

    def pass_c(k, j, h):
        ref = rows.at[at.c, piece(k, j, h), :]
        send(ref, ref, c_sems.at[0, k, j, h], c_sems.at[1, k, j, h], at.other_core())

    own_hot = hot[at.z, 0:cap, :]
    rows[at.c, 0:cap, :] = dot(own_hot, src[at.c], ((1,), (0,))).astype(bf16)
    for h in range(PIECES):
        pass_x(0, h)
    for m in range(LINE - 1):
        pack[m] = dot(
            hot[at.lines[m], 0:cap, :], src[at.c, :, window], ((1,), (0,))
        ).astype(bf16)
        for h in range(PIECES):
            send(
                pack.at[m, pl.ds(h * size, size), :],
                rows.at[at.c, pl.ds(pl.multiple_of(at.slots[m] * BLOCKS * cap + h * size, 16), size), window],
                z_sems.at[0, m, h], z_sems.at[1, at.slots[m], h], at.along(at.lines[m]),
            )

    router = router_ref[...]
    logits = dot(router.astype(bf16), src[0], ((1,), (1,)))
    chosen = [
        jnp.sum(jnp.where(mask, logits, 0.0), axis=0, keepdims=True)
        for mask in (is_first, is_second)
    ]
    margin = chosen[0] - chosen[1]
    weights = [jax.nn.sigmoid(margin), jax.nn.sigmoid(-margin)]
    sent = [w.astype(bf16).astype(f32) for w in weights]
    by_expert = jnp.where(is_first, sent[0], 0.0) + jnp.where(is_second, sent[1], 0.0)
    for m, z in enumerate((at.z,) + at.lines):
        gate_send[m] = dot(by_expert.astype(bf16), hot[z], ((1,), (1,)))
    gate_recv[0] = gate_send[0]
    send(gate_send.at[0], gate_recv.at[1], gx_sems.at[0, 0], gx_sems.at[1, 0], at.across())
    for m in range(LINE - 1):
        send(
            gate_send.at[m + 1], gate_recv.at[at.slots[m] * BLOCKS],
            gz_sems.at[0, m], gz_sems.at[1, at.slots[m]], at.along(at.lines[m]),
        )
    rows[1 - at.c, 0:cap, :] = dot(own_hot, src[1 - at.c], ((1,), (0,))).astype(bf16)
    g_sum[...] = jnp.zeros_like(g_sum)

    row_id = lax.broadcasted_iota(jnp.int32, (side, side), 0)
    lane_id = lax.broadcasted_iota(jnp.int32, (side, side), 1)
    top8 = lax.broadcasted_iota(jnp.int32, (8, side), 0)
    diagonal = row_id == lane_id

    def to_column(row):
        return jnp.sum(jnp.where(diagonal, row, 0.0), axis=1, keepdims=True)

    def take_row(tile, index):
        return jnp.sum(jnp.where(top8 == index, tile, 0.0), axis=0, keepdims=True)

    sources = (at.z,) + at.lines

    def step_z(k):
        for h in range(PIECES):
            arrived(rows.at[at.c, piece(k, 0, h), window], z_sems.at[1, k, h])
            pass_x(k, h)
            pass_y(k, 0, h)
        arrived(gate_recv.at[k * BLOCKS], gz_sems.at[1, k])
        send(
            gate_recv.at[k * BLOCKS], gate_recv.at[k * BLOCKS + 1],
            gx_sems.at[0, k], gx_sems.at[1, k], at.across(),
        )

    def step_x(k):
        for h in range(PIECES):
            arrived(rows.at[at.c, piece(k, 1, h), window], x_sems.at[1, k, h])
            pass_y(k, 1, h)

    def step_y(k, j):
        for h in range(PIECES):
            arrived(rows.at[at.c, piece(k, j, h), inner], y_sems.at[1, k, j, h])
            pass_c(k, j, h)

    def forward(k):
        arrived(gate_recv.at[k * BLOCKS + 1], gx_sems.at[1, k])
        for j in range(BLOCKS):
            column = to_column(take_row(gate_recv[k * BLOCKS + j], at.z))
            base = (k * BLOCKS + j) * cap
            gate_col[base : base + cap, :] = jnp.broadcast_to(column[0:cap], (cap, side))
        for j in range(BLOCKS):
            if (k, j) != (0, 0):
                for h in range(PIECES):
                    arrived(rows.at[1 - at.c, piece(k, j, h), :], c_sems.at[1, k, j, h])
        if k == 0:
            for copy in loads[2:]:
                copy.wait()
        both = dot(rows[0, chunk(k), :], wgu[...], ((1,), (0,)))
        pre_gate, pre_up = both[:, :hidden], both[:, hidden:]
        back = dot(rows[1, chunk(k), :], wd[...], ((1,), (1,)))
        gate = gate_col[chunk(k), 0:1]
        sig = jax.nn.sigmoid(pre_gate)
        active = pre_gate * sig
        product = active * pre_up
        terms = jnp.sum(product.astype(bf16).astype(f32) * back, axis=1, keepdims=True)
        scaled = gate * back
        dgu[chunk(k), 0:hidden] = (scaled * pre_up * sig * (1.0 + pre_gate * (1.0 - sig))).astype(bf16)
        dgu[chunk(k), hidden:] = (scaled * active).astype(bf16)
        hs[chunk(k), :] = (gate * product).astype(bf16)
        for j in range(BLOCKS):
            line = jnp.sum(
                jnp.where(diagonal[0:cap], terms[j * cap : (j + 1) * cap], 0.0),
                axis=0, keepdims=True,
            )
            block = sources[k] * BLOCKS + (at.x if j == 0 else 1 - at.x)
            g_sum[...] += jnp.where(top8 == block, line, 0.0)

    def input_grad(k, plane, core):
        begin = pl.multiple_of((plane * CORES + core) * part, part)
        return dot(dgu[chunk(k), :], wgu[pl.ds(begin, part), :], ((1,), (1,)))

    def backward(k):
        for p in range(PLANES):
            dx_send[k, p] = input_grad(k, p, 1 - at.c).astype(bf16)
            send(
                dx_send.at[k, p], c_recv.at[k, p],
                sc_sems.at[0, k, p], sc_sems.at[1, k, p], at.other_core(),
            )
        for n, plane in enumerate((1 - at.y, at.y)):
            dx_own[k, n] = input_grad(k, plane, at.c)

    def after_c(k):
        for p in range(PLANES):
            arrived(c_recv.at[k, p], sc_sems.at[1, k, p])
        for j in (1, 0):
            part_rows = slice(j * cap, (j + 1) * cap)
            y_send[k, j] = (
                dx_own[k, 0, part_rows, :] + c_recv[k, 1 - at.y, part_rows, :].astype(f32)
            ).astype(bf16)
            send(
                y_send.at[k, j], y_recv.at[k, j],
                sy_sems.at[0, k, j], sy_sems.at[1, k, j], at.other_plane(),
            )
        for j in (1, 0):
            part_rows = slice(j * cap, (j + 1) * cap)
            y_own[k, j] = dx_own[k, 1, part_rows, :] + c_recv[k, at.y, part_rows, :].astype(f32)

    def after_y(k):
        arrived(y_recv.at[k, 1], sy_sems.at[1, k, 1])
        x_send[k] = (y_own[k, 1] + y_recv[k, 1].astype(f32)).astype(bf16)
        send(x_send.at[k], x_recv.at[k], sx_sems.at[0, k], sx_sems.at[1, k], at.across())
        arrived(y_recv.at[k, 0], sy_sems.at[1, k, 0])
        y_own[k, 0] = y_own[k, 0] + y_recv[k, 0].astype(f32)

    def after_x(k):
        arrived(x_recv.at[k], sx_sems.at[1, k])
        total = (y_own[k, 0] + x_recv[k].astype(f32)).astype(bf16)
        if k == 0:
            z_recv[at.z] = total
            return
        z_send[k - 1] = total
        mine = 1 if k == 1 else at.rank
        send(
            z_send.at[k - 1], z_recv.at[at.z],
            sz_sems.at[0, k], sz_sems.at[1, mine], at.along(sources[k]),
        )

    stages = (at.other_core, at.other_plane, at.across)

    def gate_stage(n):
        if n > 0:
            arrived(g_recv.at[n - 1], gp_sems.at[1, n - 1])
            g_sum[...] += g_recv[n - 1]
        if n < len(stages):
            g_send[n] = g_sum[...]
            send(g_send.at[n], g_recv.at[n], gp_sems.at[0, n], gp_sems.at[1, n], stages[n]())
            return
        g_send[n] = g_sum[...]
        gz_recv[at.z] = g_sum[...]
        for m in range(LINE - 1):
            send(
                g_send.at[n], gz_recv.at[at.z],
                gl_sems.at[0, m], gl_sems.at[1, at.slots[m]], at.along(at.lines[m]),
            )

    state = {}

    def split3(value):
        high = value.astype(bf16).astype(f32)
        middle = (value - high).astype(bf16).astype(f32)
        low = (value - high - middle).astype(bf16).astype(f32)
        return jnp.concatenate([high, middle, low, jnp.zeros_like(value)], axis=0).astype(bf16)

    def gate_finish():
        for m in range(LINE - 1):
            arrived(gz_recv.at[at.lines[m]], gl_sems.at[1, m + 1])
        own = at.z * BLOCKS + at.x
        grads = [jnp.zeros((1, tok_rows), f32)] * 2
        for e in range(LINE):
            column = to_column(take_row(gz_recv[e], own))
            term = jnp.sum(column * hot[e].astype(f32), axis=0, keepdims=True)
            grads[0] = grads[0] + jnp.where(first == e, term, 0.0)
            grads[1] = grads[1] + jnp.where(second == e, term, 0.0)
        gg_ref[...] = jnp.where(row8 == 0, grads[0], jnp.where(row8 == 1, grads[1], 0.0))
        lead = weights[0] * weights[1] * (grads[0] - grads[1])
        logit_grad = jnp.where(is_first, lead, 0.0) - jnp.where(is_second, lead, 0.0)
        state["parts"] = split3(logit_grad)
        sums = dot(state["parts"], src[0], ((1,), (0,)))
        r_send[...] = sums[0:8] + sums[8:16] + sums[16:24]
        wide = r_send.shape[1] // (LINE * BLOCKS)
        for step in range(LINE):
            for flip in range(BLOCKS):
                z, x = (at.z + step) % LINE, (at.x + flip) % BLOCKS
                columns = pl.ds(pl.multiple_of((z * BLOCKS + x) * wide, wide), wide)
                n = step * BLOCKS + flip
                if n == 0:
                    r_recv[0] = r_send[:, columns]
                    continue
                send(
                    r_send.at[:, columns], r_recv.at[n],
                    r_sems.at[0, n], r_sems.at[1, n], at.device(z, x),
                )

    def token_finish():
        begin = pl.multiple_of(at.tp * part, part)
        columns = router_ref[:, pl.ds(begin, part)]
        triple = jnp.concatenate([columns] * 3 + [jnp.zeros_like(columns)], axis=0).astype(bf16)
        total = dot(state["parts"], triple, ((0,), (0,)))
        for m in range(LINE - 1):
            arrived(z_recv.at[at.lines[m]], sz_sems.at[1, m + 1])
        for e in range(LINE):
            total = total + dot(hot[e, 0:cap, :], z_recv[e], ((0,), (0,)))
        tg_ref[...] = total.astype(bf16)

    def router_finish():
        total = r_recv[0]
        for n in range(1, LINE * BLOCKS):
            arrived(r_recv.at[n], r_sems.at[1, n])
            total = total + r_recv[n]
        rg_ref[...] = total

    tile = 256

    def weight_grads(n):
        if n < 2:
            half = width // tile // 2

            @pl.loop(n * half, (n + 1) * half)
            def _(m):
                columns = pl.ds(pl.multiple_of(m * tile, tile), tile)
                both = dot(rows[0, :, columns], dgu[...], ((0,), (0,))).astype(bf16)
                gw_ref[columns, :] = both[:, :hidden]
                gu_ref[columns, :] = both[:, hidden:]

            return

        @pl.loop(0, width // tile)
        def _(m):
            columns = pl.ds(pl.multiple_of(m * tile, tile), tile)
            gd_ref[:, columns] = dot(hs[...], rows[1, :, columns], ((0,), (0,))).astype(bf16)

    steps = {
        "X": step_x, "Z": step_z, "Y": step_y, "F": forward, "D": backward, "A": after_c,
        "B": after_y, "E": after_x, "W": weight_grads, "T": token_finish, "R": router_finish,
    }
    for token in SCHEDULE:
        numbers = [int(digit) for digit in token[1:]]
        if token[0] == "G":
            gate_stage(*numbers) if numbers[0] <= len(stages) else gate_finish()
        else:
            steps[token[0]](*numbers)
    for copy in started:
        copy.wait_send()


def fused_shards(tokens, cotangent, routes, router, w_gate, w_up, w_down):
    ep_count, tp_count = lax.axis_size("ep"), lax.axis_size("tp")
    experts = ep_count // BLOCKS
    tok_rows, width = tokens.shape
    cap = 3 * tok_rows * routes.shape[1] // (2 * experts)
    part, hidden = width // tp_count, w_down.shape[1]
    span = 5 * width // 8
    seg = width // (ep_count * tp_count)
    routes_t = jnp.pad(routes.T, ((0, 8 - routes.shape[1]), (0, 0)))
    router_t = jnp.pad(router.T.astype(jnp.float32), ((0, 8 - experts), (0, 0)))
    dma = pltpu.SemaphoreType.DMA
    bf16, f32 = jnp.bfloat16, jnp.float32
    vmem = pl.BlockSpec(memory_space=pltpu.VMEM)
    anywhere = pl.BlockSpec(memory_space=pl.ANY)
    total, pair = ep_count * cap, BLOCKS * cap
    tiny = (8, 128)
    token_grad, gates, grad_gate, grad_up, grad_down, router_grad = pl.pallas_call(
        fused_kernel,
        out_shape=(
            jax.ShapeDtypeStruct((tok_rows, part), bf16),
            jax.ShapeDtypeStruct((8, tok_rows), f32),
            jax.ShapeDtypeStruct((width, hidden), bf16),
            jax.ShapeDtypeStruct((width, hidden), bf16),
            jax.ShapeDtypeStruct((hidden, width), bf16),
            jax.ShapeDtypeStruct((8, width // ep_count), f32),
        ),
        in_specs=[anywhere, anywhere, vmem, vmem, anywhere, anywhere, anywhere],
        out_specs=[vmem] * 6,
        scratch_shapes=[
            pltpu.VMEM((2, tok_rows, width), bf16),
            pltpu.VMEM((width, 2 * hidden), bf16),
            pltpu.VMEM((hidden, width), bf16),
            pltpu.VMEM((2, total, width), bf16),
            pltpu.VMEM((LINE - 1, cap, span), bf16),
            pltpu.VMEM((LINE, 128, tok_rows), bf16),
            pltpu.VMEM((LINE,) + tiny, f32),
            pltpu.VMEM((ep_count,) + tiny, f32),
            pltpu.VMEM((total, 128), f32),
            pltpu.VMEM((total, hidden), bf16),
            pltpu.VMEM((total, 2 * hidden), bf16),
            pltpu.VMEM((LINE, PLANES, pair, part), bf16),
            pltpu.VMEM((LINE, PLANES, pair, part), f32),
            pltpu.VMEM((LINE, PLANES, pair, part), bf16),
            pltpu.VMEM((LINE, BLOCKS, cap, part), bf16),
            pltpu.VMEM((LINE, BLOCKS, cap, part), bf16),
            pltpu.VMEM((LINE, BLOCKS, cap, part), f32),
            pltpu.VMEM((LINE, cap, part), bf16),
            pltpu.VMEM((LINE, cap, part), bf16),
            pltpu.VMEM((LINE - 1, cap, part), bf16),
            pltpu.VMEM((LINE, cap, part), bf16),
            pltpu.VMEM(tiny, f32),
            pltpu.VMEM((4,) + tiny, f32),
            pltpu.VMEM((3,) + tiny, f32),
            pltpu.VMEM((LINE,) + tiny, f32),
            pltpu.VMEM((8, width), f32),
            pltpu.VMEM((ep_count, 8, width // ep_count), f32),
            dma((5,)),
            dma((2, LINE, PIECES)),
            dma((2, LINE, PIECES)),
            dma((2, LINE, BLOCKS, PIECES)),
            dma((2, LINE, BLOCKS, PIECES)),
            dma((2, LINE)),
            dma((2, LINE)),
            dma((2, LINE, PLANES)),
            dma((2, LINE, BLOCKS)),
            dma((2, LINE)),
            dma((2, LINE)),
            dma((2, 3)),
            dma((2, LINE)),
            dma((2, ep_count)),
        ],
        compiler_params=pltpu.CompilerParams(
            collective_id=0, has_side_effects=True, vmem_limit_bytes=60 * 1024 * 1024
        ),
    )(tokens, cotangent, routes_t, router_t, w_gate[0], w_up[0], w_down[0])
    own = lax.dynamic_slice_in_dim(router_grad, lax.axis_index("tp") * seg, seg, 1)
    return (
        token_grad,
        gates[: routes.shape[1]].T,
        grad_gate[None],
        grad_up[None],
        grad_down[None],
        own[:experts].T,
    )


def shards(tokens, cotangent, routes, router, w_gate, w_up, w_down):
    grid = (lax.axis_size("ep"), lax.axis_size("tp"))
    path = fused_shards if grid == (LINE * BLOCKS, PLANES * CORES) else routed_shards
    return path(tokens, cotangent, routes, router, w_gate, w_up, w_down)


def solution(mesh):
    placed = (
        P("ep", None),
        P("ep", None),
        P("ep", None),
        P(),
        P("ep", None, "tp"),
        P("ep", None, "tp"),
        P("ep", "tp", None),
    )
    return jax.shard_map(
        shards,
        mesh=mesh,
        in_specs=placed,
        out_specs=(
            P("ep", "tp"),
            P("ep", None),
            P("ep", None, "tp"),
            P("ep", None, "tp"),
            P("ep", "tp", None),
            P(("ep", "tp"), None),
        ),
        check_vma=False,
    )
```

time: 161 us -> 98.9 us (0.61)
  matrix products: 33.8 us -> 0 us
  blocking collectives: 22.4 us -> 0 us
  Pallas kernels: 99.6 us -> 84.2 us
  local copies, waits for them, and re-layouts: 1.69 us -> 12.3 us
    dot_general x11 -> x0, matrix products: 33.8 us -> none  [the longest x1 4.36 us: dense_shards(): lax.dot_general(d_up, w_up, contract_hidden, preferred_element_type=jnp.f...]
    all_gather x1 -> x0, blocking collectives: 22.4 us -> none  [dense_shards(): lax.all_gather(routes.T.astype(jnp.float32), 'ep', axis=1, tiled=True)]
    pallas_call x2 -> x1, Pallas kernels: 99.6 us -> 84.2 us  [fused_shards(): pl.pallas_call(fused_kernel, out_shape=(jax.ShapeDtypeStruct((tok_rows, p...]
    unnamed x10 -> x8, local copies, waits for them, and re-layouts: 0.44 us -> 8.43 us
where the time goes in v1:
time: 98.9 us; the launch traced here: 98.5 us
  Pallas kernels  84.2 us (85%)
  local copies, waits for them, and re-layouts  12.3 us (12%)
  other arithmetic  1.35 us (1%)
    pallas_call x1, Pallas kernels, fused_shards(): pl.pallas_call(fused_kernel, out_shape=(jax.ShapeDtypeStruct((tok_rows, p...  84.2 us
    unnamed x8, local copies, waits for them, and re-layouts  8.43 us

profile of v1, /device:TPU:0, one launch (start us, length us, event | category | flops | bytes accessed | tf_op | source)
XLA Modules:
  0.0 98.5 jit_solution(6296361567086112975)
XLA Ops:
  0.6 1.3 %pad.10.routes_ref = s32[8,128]{1,0:T(8,128)} pad(s32[2,128]{1,0:T(2,128)} %bitcast.19, s32[]{:T(128)} %constant.3.clone.1), padding=0_6x0_0 | pad | bytes 5124 | tf_op jit(solution)/shard_map/jit(_pad)/pad | solution.py:571
  1.9 1.4 %pad_convert_fusion.router_ref = f32[8,2048]{1,0:T(8,128)} fusion(bf16[4,2048]{1,0:T(4,128)(2,1)} %bitcast.18), kind=kLoop, calls=%fused_computation | loop fusion | flops 16384 | bytes 81920 | tf_op jit(solution)/shard_map/jit(_pad)/pad | solution.py:572
  3.3 84.2 %shard_map.118 = (bf16[128,512]{1,0:T(8,128)(2,1)}, f32[8,128]{1,0:T(8,128)}, bf16[2048,512]{1,0:T(8,128)(2,1)}, bf16[2048,512]{1,0:T(8,128)(2,1)}, bf16[512,2048]{1,0:T(8,128)(2,1)}, /*index=5*/f32[8,256]{1,0:T(8,128)}) custom-call(bf16[128,2048]{1,0:T(8,128)(2,1)} %tok_hbm.1, bf16[128,2048]{1,0:T(8,128)(2,1)} %cot_hbm.1, s32[8,128]{1,0:T(8,128)} %pad.10.routes_ref, ...), custom_call_target="tpu_custom_call" | custom-call | tf_op jit(solution)/shard_map/pallas_call | solution.py:579
  87.5 1.2 %slice_bitcast_fusion.1 = f32[128,2]{0,1:T(2,128)} fusion(f32[8,128]{1,0:T(8,128)} %get-tuple-element.13), kind=kLoop, calls=%fused_computation.2 | loop fusion | bytes 2048 | tf_op jit(solution)/shard_map/transpose | solution.py:641
  88.7 0.8 constant_dynamic-slice_fusion
  89.5 0.6 slice_bitcast_fusion
  90.1 1.6 %copy.17 = bf16[128,512]{1,0:T(8,128)(2,1)} copy(bf16[128,512]{1,0:T(8,128)(2,1)} %get-tuple-element.24) | data formatting | bytes 262144
  91.6 0.0 copy-start.1
  91.6 3.2 %copy.18 = bf16[1,2048,512]{2,1,0:T(8,128)(2,1)} copy(bf16[1,2048,512]{2,1,0:T(8,128)(2,1)} %bitcast.17) | data formatting | bytes 4194304
  94.8 0.0 copy-done.1
  94.8 0.0 copy-start
  94.8 1.3 %copy.19 = bf16[1,2048,512]{2,1,0:T(8,128)(2,1)} copy(bf16[1,2048,512]{2,1,0:T(8,128)(2,1)S(1)} %bitcast.16) | data formatting | bytes 4194304
  96.2 1.0 %copy-done = bf16[512,2048]{1,0:T(8,128)(2,1)S(1)} copy-done((bf16[512,2048]{1,0:T(8,128)(2,1)S(1)}, bf16[512,2048]{1,0:T(8,128)(2,1)}, u32[]{:S(2)}) %copy-start) | copy-done | bytes 2097176
  97.2 1.3 %copy.20 = bf16[1,512,2048]{2,1,0:T(8,128)(2,1)} copy(bf16[1,512,2048]{2,1,0:T(8,128)(2,1)S(1)} %bitcast.15) | data formatting | bytes 4194304
Async XLA Ops:
  91.6 3.2 %copy-start.1 = (bf16[2048,512]{1,0:T(8,128)(2,1)S(1)}, bf16[2048,512]{1,0:T(8,128)(2,1)}, u32[]{:S(2)}) copy-start(bf16[2048,512]{1,0:T(8,128)(2,1)} %get-tuple-element.15) | copy-start | bytes 6291460
  94.8 2.3 %copy-start = (bf16[512,2048]{1,0:T(8,128)(2,1)S(1)}, bf16[512,2048]{1,0:T(8,128)(2,1)}, u32[]{:S(2)}) copy-start(bf16[512,2048]{1,0:T(8,128)(2,1)} %get-tuple-element.16) | copy-start | bytes 6291460

commit v2 on v1

--- a/solution.py
+++ b/solution.py
@@ -10,6 +10,8 @@
 PLANES = 2
 LINE = 4
 PIECES = 2
+SIXTEENTHS = 10
+VMEM_LIMIT = 40 * 1024 * 1024
 MESH = pl.DeviceIdType.MESH
 
 
@@ -193,33 +195,36 @@
     def other_core(self):
         return {"ep": self.z * BLOCKS + self.x, "tp": self.y * CORES + 1 - self.c}
 
-    def turned(self, step, flip):
-        return self.device((self.z + step) % LINE, (self.x + flip) % BLOCKS)
-
-    def greet(self):
-        barrier = pltpu.get_barrier_semaphore()
-        peers = [self.turned(step, flip) for step in range(LINE) for flip in range(2)][1:]
-        peers += [self.other_plane(), self.other_core()]
+    def diagonal(self):
+        return {"ep": self.z * BLOCKS + 1 - self.x, "tp": (1 - self.y) * CORES + self.c}
+
+    def announce(self):
+        peers = [self.along(z) for z in self.lines]
+        peers += [self.across(), self.other_plane(), self.diagonal(), self.other_core()]
         for peer in peers:
-            pl.semaphore_signal(barrier, inc=1, device_id=peer, device_id_type=MESH)
-        pl.semaphore_wait(barrier, len(peers))
+            pl.semaphore_signal(
+                pltpu.get_barrier_semaphore(), inc=1, device_id=peer, device_id_type=MESH
+            )
+        return len(peers)
 
 
 SCHEDULE = (
-    "X0", "Z1", "Y01", "Y10", "F0", "X1", "Z2", "Y11", "D0", "Y20", "A0", "F1", "X2", "Z3",
-    "B0", "D1", "Y21", "Y30", "E0", "A1", "X3", "F2", "B1", "D2", "Y31", "E1", "A2", "F3", "G0",
-    "D3", "G1", "B2", "A3", "G2", "E2", "W0", "B3", "G3", "W1", "E3", "W2", "G4", "T", "R",
+    "X00", "Z10", "Z11", "X01", "X10", "Z20", "Y010", "Y011", "X11", "Z21", "X20", "Z30", "F0",
+    "Y101", "X21", "D0", "Y110", "Z31", "Y201", "Y100", "A0", "Y111", "Y211", "Y200", "F1",
+    "X30", "X31", "Y210", "Y300", "D1", "F2", "Y301", "A1", "D2", "Y310", "Y311", "A2", "F3",
+    "G0", "D3", "E0", "E1", "G1", "A3", "W0", "G2", "E2", "W1", "E3", "G3", "R0", "W2", "T",
+    "R1",
 )
 
 
 def fused_kernel(
-    tok_hbm, cot_hbm, routes_ref, router_ref, wg_hbm, wu_hbm, wd_hbm,
+    tok_hbm, cot_hbm, routes_hbm, router_hbm, wg_hbm, wu_hbm, wd_hbm,
     tg_ref, gg_ref, gw_ref, gu_ref, gd_ref, rg_ref,
     src, wgu, wd, rows, pack, hot, gate_send, gate_recv, gate_col,
-    hs, dgu, dx_send, dx_own, c_recv, y_send, y_recv, y_own, x_send, x_recv, z_send, z_recv,
-    g_sum, g_send, g_recv, gz_recv, r_send, r_recv,
+    routes_ref, router_ref, router_all, hs, dgu, dx_send, dx_own, c_recv, s_send, s_recv, s_own, z_send, z_recv,
+    g_sum, g_send, g_recv, gz_recv, r_send, r_recv, rz_send, rz_recv,
     load_sems, z_sems, x_sems, y_sems, c_sems, gz_sems, gx_sems,
-    sc_sems, sy_sems, sx_sems, sz_sems, gp_sems, gl_sems, r_sems,
+    sc_sems, s_sems, sz_sems, gp_sems, gl_sems, r_sems,
 ):
     f32, bf16 = jnp.float32, jnp.bfloat16
     at = Place()
@@ -250,15 +255,19 @@
             device_id=at.across(), device_id_type=MESH,
         ).wait_recv()
 
+    greeted = at.announce()
     loads = [
+        pltpu.make_async_copy(routes_hbm, routes_ref, load_sems.at[5]),
         pltpu.make_async_copy(tok_hbm, src.at[0], load_sems.at[0]),
         pltpu.make_async_copy(cot_hbm, src.at[1], load_sems.at[1]),
+        pltpu.make_async_copy(router_hbm, router_ref, load_sems.at[6]),
         pltpu.make_async_copy(wg_hbm, wgu.at[:, pl.ds(0, hidden)], load_sems.at[2]),
         pltpu.make_async_copy(wu_hbm, wgu.at[:, pl.ds(hidden, hidden)], load_sems.at[3]),
         pltpu.make_async_copy(wd_hbm, wd, load_sems.at[4]),
     ]
     for copy in loads:
         copy.start()
+    loads[0].wait()
 
     side = hot.shape[1]
     row8 = lax.broadcasted_iota(jnp.int32, (8, tok_rows), 0)
@@ -273,10 +282,8 @@
     slot = (lax.broadcasted_iota(jnp.int32, (side, tok_rows), 0) + 1).astype(f32)
     for e in range(LINE):
         hot[e] = jnp.where(slot == place[e : e + 1, :], 1.0, 0.0).astype(bf16)
-    at.greet()
-
-    loads[0].wait()
     loads[1].wait()
+    loads[2].wait()
 
     def piece(k, j, h):
         return pl.ds((k * BLOCKS + j) * cap + h * size, size)
@@ -300,21 +307,27 @@
 
     own_hot = hot[at.z, 0:cap, :]
     rows[at.c, 0:cap, :] = dot(own_hot, src[at.c], ((1,), (0,))).astype(bf16)
-    for h in range(PIECES):
-        pass_x(0, h)
     for m in range(LINE - 1):
         pack[m] = dot(
             hot[at.lines[m], 0:cap, :], src[at.c, :, window], ((1,), (0,))
         ).astype(bf16)
+    pl.semaphore_wait(pltpu.get_barrier_semaphore(), greeted)
+    for h in range(PIECES):
+        pass_x(0, h)
+    for m in range(LINE - 1):
         for h in range(PIECES):
+            begin = pl.multiple_of(at.slots[m] * BLOCKS * cap + h * size, 16)
             send(
                 pack.at[m, pl.ds(h * size, size), :],
-                rows.at[at.c, pl.ds(pl.multiple_of(at.slots[m] * BLOCKS * cap + h * size, 16), size), window],
+                rows.at[at.c, pl.ds(begin, size), window],
                 z_sems.at[0, m, h], z_sems.at[1, at.slots[m], h], at.along(at.lines[m]),
             )
 
-    router = router_ref[...]
-    logits = dot(router.astype(bf16), src[0], ((1,), (1,)))
+    experts = router_ref.shape[0]
+    loads[3].wait()
+    router_all[0:experts, :] = router_ref[...].astype(f32)
+    router_all[experts:, :] = jnp.zeros((8 - experts, width), f32)
+    logits = dot(router_all[...].astype(bf16), src[0], ((1,), (1,)))
     chosen = [
         jnp.sum(jnp.where(mask, logits, 0.0), axis=0, keepdims=True)
         for mask in (is_first, is_second)
@@ -348,26 +361,24 @@
 
     sources = (at.z,) + at.lines
 
-    def step_z(k):
-        for h in range(PIECES):
-            arrived(rows.at[at.c, piece(k, 0, h), window], z_sems.at[1, k, h])
-            pass_x(k, h)
-            pass_y(k, 0, h)
-        arrived(gate_recv.at[k * BLOCKS], gz_sems.at[1, k])
-        send(
-            gate_recv.at[k * BLOCKS], gate_recv.at[k * BLOCKS + 1],
-            gx_sems.at[0, k], gx_sems.at[1, k], at.across(),
-        )
-
-    def step_x(k):
-        for h in range(PIECES):
-            arrived(rows.at[at.c, piece(k, 1, h), window], x_sems.at[1, k, h])
-            pass_y(k, 1, h)
-
-    def step_y(k, j):
-        for h in range(PIECES):
-            arrived(rows.at[at.c, piece(k, j, h), inner], y_sems.at[1, k, j, h])
-            pass_c(k, j, h)
+    def step_z(k, h):
+        arrived(rows.at[at.c, piece(k, 0, h), window], z_sems.at[1, k, h])
+        pass_x(k, h)
+        pass_y(k, 0, h)
+        if h == 0:
+            arrived(gate_recv.at[k * BLOCKS], gz_sems.at[1, k])
+            send(
+                gate_recv.at[k * BLOCKS], gate_recv.at[k * BLOCKS + 1],
+                gx_sems.at[0, k], gx_sems.at[1, k], at.across(),
+            )
+
+    def step_x(k, h):
+        arrived(rows.at[at.c, piece(k, 1, h), window], x_sems.at[1, k, h])
+        pass_y(k, 1, h)
+
+    def step_y(k, j, h):
+        arrived(rows.at[at.c, piece(k, j, h), inner], y_sems.at[1, k, j, h])
+        pass_c(k, j, h)
 
     def forward(k):
         arrived(gate_recv.at[k * BLOCKS + 1], gx_sems.at[1, k])
@@ -380,7 +391,7 @@
                 for h in range(PIECES):
                     arrived(rows.at[1 - at.c, piece(k, j, h), :], c_sems.at[1, k, j, h])
         if k == 0:
-            for copy in loads[2:]:
+            for copy in loads[4:]:
                 copy.wait()
         both = dot(rows[0, chunk(k), :], wgu[...], ((1,), (0,)))
         pre_gate, pre_up = both[:, :hidden], both[:, hidden:]
@@ -419,29 +430,27 @@
     def after_c(k):
         for p in range(PLANES):
             arrived(c_recv.at[k, p], sc_sems.at[1, k, p])
-        for j in (1, 0):
+
+        def summed(n, plane, j):
             part_rows = slice(j * cap, (j + 1) * cap)
-            y_send[k, j] = (
-                dx_own[k, 0, part_rows, :] + c_recv[k, 1 - at.y, part_rows, :].astype(f32)
-            ).astype(bf16)
+            return dx_own[k, n, part_rows, :] + c_recv[k, plane, part_rows, :].astype(f32)
+
+        ways = (
+            (0, 1 - at.y, 1, at.diagonal), (1, at.y, 1, at.across), (0, 1 - at.y, 0, at.other_plane),
+        )
+        for i, (n, plane, j, peer) in enumerate(ways):
+            s_send[k, i] = summed(n, plane, j).astype(bf16)
             send(
-                y_send.at[k, j], y_recv.at[k, j],
-                sy_sems.at[0, k, j], sy_sems.at[1, k, j], at.other_plane(),
+                s_send.at[k, i], s_recv.at[k, i], s_sems.at[0, k, i], s_sems.at[1, k, i], peer()
             )
-        for j in (1, 0):
-            part_rows = slice(j * cap, (j + 1) * cap)
-            y_own[k, j] = dx_own[k, 1, part_rows, :] + c_recv[k, at.y, part_rows, :].astype(f32)
-
-    def after_y(k):
-        arrived(y_recv.at[k, 1], sy_sems.at[1, k, 1])
-        x_send[k] = (y_own[k, 1] + y_recv[k, 1].astype(f32)).astype(bf16)
-        send(x_send.at[k], x_recv.at[k], sx_sems.at[0, k], sx_sems.at[1, k], at.across())
-        arrived(y_recv.at[k, 0], sy_sems.at[1, k, 0])
-        y_own[k, 0] = y_own[k, 0] + y_recv[k, 0].astype(f32)
+        s_own[k] = summed(1, at.y, 0)
 
     def after_x(k):
-        arrived(x_recv.at[k], sx_sems.at[1, k])
-        total = (y_own[k, 0] + x_recv[k].astype(f32)).astype(bf16)
+        total = s_own[k]
+        for i in range(3):
+            arrived(s_recv.at[k, i], s_sems.at[1, k, i])
+            total = total + s_recv[k, i].astype(f32)
+        total = total.astype(bf16)
         if k == 0:
             z_recv[at.z] = total
             return
@@ -452,23 +461,28 @@
             sz_sems.at[0, k], sz_sems.at[1, mine], at.along(sources[k]),
         )
 
-    stages = (at.other_core, at.other_plane, at.across)
-
     def gate_stage(n):
-        if n > 0:
-            arrived(g_recv.at[n - 1], gp_sems.at[1, n - 1])
-            g_sum[...] += g_recv[n - 1]
-        if n < len(stages):
-            g_send[n] = g_sum[...]
-            send(g_send.at[n], g_recv.at[n], gp_sems.at[0, n], gp_sems.at[1, n], stages[n]())
-            return
-        g_send[n] = g_sum[...]
-        gz_recv[at.z] = g_sum[...]
-        for m in range(LINE - 1):
-            send(
-                g_send.at[n], gz_recv.at[at.z],
-                gl_sems.at[0, m], gl_sems.at[1, at.slots[m]], at.along(at.lines[m]),
-            )
+        if n == 0:
+            send(g_sum, g_recv.at[0], gp_sems.at[0, 0], gp_sems.at[1, 0], at.other_core())
+        elif n == 1:
+            arrived(g_recv.at[0], gp_sems.at[1, 0])
+            g_send[0] = g_sum[...] + g_recv[0]
+            for i, peer in enumerate((at.across, at.other_plane, at.diagonal), 1):
+                send(g_send.at[0], g_recv.at[i], gp_sems.at[0, i], gp_sems.at[1, i], peer())
+        elif n == 2:
+            total = g_send[0]
+            for i in range(1, 4):
+                arrived(g_recv.at[i], gp_sems.at[1, i])
+                total = total + g_recv[i]
+            g_send[1] = total
+            gz_recv[at.z] = total
+            for m in range(LINE - 1):
+                send(
+                    g_send.at[1], gz_recv.at[at.z],
+                    gl_sems.at[0, m], gl_sems.at[1, at.slots[m]], at.along(at.lines[m]),
+                )
+        else:
+            gate_finish()
 
     state = {}
 
@@ -493,24 +507,17 @@
         logit_grad = jnp.where(is_first, lead, 0.0) - jnp.where(is_second, lead, 0.0)
         state["parts"] = split3(logit_grad)
         sums = dot(state["parts"], src[0], ((1,), (0,)))
-        r_send[...] = sums[0:8] + sums[8:16] + sums[16:24]
-        wide = r_send.shape[1] // (LINE * BLOCKS)
-        for step in range(LINE):
-            for flip in range(BLOCKS):
-                z, x = (at.z + step) % LINE, (at.x + flip) % BLOCKS
-                columns = pl.ds(pl.multiple_of((z * BLOCKS + x) * wide, wide), wide)
-                n = step * BLOCKS + flip
-                if n == 0:
-                    r_recv[0] = r_send[:, columns]
-                    continue
-                send(
-                    r_send.at[:, columns], r_recv.at[n],
-                    r_sems.at[0, n], r_sems.at[1, n], at.device(z, x),
-                )
+        sums = sums[0:8] + sums[8:16] + sums[16:24]
+        wide = r_send.shape[3]
+        for z in range(LINE):
+            for x in range(BLOCKS):
+                begin = (z * BLOCKS + x) * wide
+                r_send[x, z] = sums[:, begin : begin + wide]
+        send(r_send.at[1 - at.x], r_recv, r_sems.at[0, 0], r_sems.at[1, 0], at.across())
 
     def token_finish():
         begin = pl.multiple_of(at.tp * part, part)
-        columns = router_ref[:, pl.ds(begin, part)]
+        columns = router_all[:, pl.ds(begin, part)]
         triple = jnp.concatenate([columns] * 3 + [jnp.zeros_like(columns)], axis=0).astype(bf16)
         total = dot(state["parts"], triple, ((0,), (0,)))
         for m in range(LINE - 1):
@@ -519,45 +526,64 @@
             total = total + dot(hot[e, 0:cap, :], z_recv[e], ((0,), (0,)))
         tg_ref[...] = total.astype(bf16)
 
-    def router_finish():
-        total = r_recv[0]
-        for n in range(1, LINE * BLOCKS):
-            arrived(r_recv.at[n], r_sems.at[1, n])
-            total = total + r_recv[n]
-        rg_ref[...] = total
+    def router_stage(n):
+        if n == 0:
+            arrived(r_recv, r_sems.at[1, 0])
+            rz_send[...] = r_send[at.x] + r_recv[...]
+            for m in range(LINE - 1):
+                send(
+                    rz_send.at[at.lines[m]], rz_recv.at[at.slots[m] - 1],
+                    r_sems.at[0, m + 1], r_sems.at[1, at.slots[m]], at.along(at.lines[m]),
+                )
+            return
+        total = rz_send[at.z]
+        for m in range(LINE - 1):
+            arrived(rz_recv.at[m], r_sems.at[1, m + 1])
+            total = total + rz_recv[m]
+        seg = rg_ref.shape[1]
+        own = jnp.zeros((8, seg), f32)
+        for i in range(PLANES * CORES):
+            own = jnp.where(at.tp == i, total[:, i * seg : (i + 1) * seg], own)
+        rg_ref[...] = own
 
     tile = 256
 
     def weight_grads(n):
         if n < 2:
             half = width // tile // 2
-
-            @pl.loop(n * half, (n + 1) * half)
-            def _(m):
-                columns = pl.ds(pl.multiple_of(m * tile, tile), tile)
+            for m in range(n * half, (n + 1) * half):
+                columns = slice(m * tile, (m + 1) * tile)
                 both = dot(rows[0, :, columns], dgu[...], ((0,), (0,))).astype(bf16)
                 gw_ref[columns, :] = both[:, :hidden]
                 gu_ref[columns, :] = both[:, hidden:]
-
             return
-
-        @pl.loop(0, width // tile)
-        def _(m):
-            columns = pl.ds(pl.multiple_of(m * tile, tile), tile)
-            gd_ref[:, columns] = dot(hs[...], rows[1, :, columns], ((0,), (0,))).astype(bf16)
+        for m in range(hidden // tile):
+            columns = slice(m * tile, (m + 1) * tile)
+            gd_ref[columns, :] = dot(hs[:, columns], rows[1], ((0,), (0,))).astype(bf16)
 
     steps = {
         "X": step_x, "Z": step_z, "Y": step_y, "F": forward, "D": backward, "A": after_c,
-        "B": after_y, "E": after_x, "W": weight_grads, "T": token_finish, "R": router_finish,
+        "E": after_x, "G": gate_stage, "W": weight_grads, "T": token_finish, "R": router_stage,
     }
     for token in SCHEDULE:
-        numbers = [int(digit) for digit in token[1:]]
-        if token[0] == "G":
-            gate_stage(*numbers) if numbers[0] <= len(stages) else gate_finish()
-        else:
-            steps[token[0]](*numbers)
+        steps[token[0]](*[int(digit) for digit in token[1:]])
     for copy in started:
         copy.wait_send()
+
+
+def store_kernel(tg_in, gg_in, gw_in, gu_in, gd_in, rg_in, tg, gg, gw, gu, gd, rg, gates, router, sems):
+    gates[...] = gg_in[0 : gates.shape[0], :]
+    router[...] = rg_in[0 : router.shape[0], :]
+    copies = []
+    for source, target in ((gw_in, gw), (gu_in, gu), (gd_in, gd), (tg_in, tg), (gates, gg), (router, rg)):
+        copies.append(pltpu.make_async_copy(source, target, sems.at[len(copies)]))
+        copies[-1].start()
+    for copy in copies:
+        copy.wait()
+
+
+def in_hbm(array):
+    return pltpu.with_memory_space_constraint(array, pltpu.HBM)
 
 
 def fused_shards(tokens, cotangent, routes, router, w_gate, w_up, w_down):
@@ -566,17 +592,15 @@
     tok_rows, width = tokens.shape
     cap = 3 * tok_rows * routes.shape[1] // (2 * experts)
     part, hidden = width // tp_count, w_down.shape[1]
-    span = 5 * width // 8
-    seg = width // (ep_count * tp_count)
-    routes_t = jnp.pad(routes.T, ((0, 8 - routes.shape[1]), (0, 0)))
-    router_t = jnp.pad(router.T.astype(jnp.float32), ((0, 8 - experts), (0, 0)))
+    span = SIXTEENTHS * width // 16
+    seg, wide = width // (ep_count * tp_count), width // ep_count
     dma = pltpu.SemaphoreType.DMA
     bf16, f32 = jnp.bfloat16, jnp.float32
     vmem = pl.BlockSpec(memory_space=pltpu.VMEM)
-    anywhere = pl.BlockSpec(memory_space=pl.ANY)
+    hbm = pl.BlockSpec(memory_space=pltpu.HBM)
     total, pair = ep_count * cap, BLOCKS * cap
     tiny = (8, 128)
-    token_grad, gates, grad_gate, grad_up, grad_down, router_grad = pl.pallas_call(
+    results = pl.pallas_call(
         fused_kernel,
         out_shape=(
             jax.ShapeDtypeStruct((tok_rows, part), bf16),
@@ -584,9 +608,9 @@
             jax.ShapeDtypeStruct((width, hidden), bf16),
             jax.ShapeDtypeStruct((width, hidden), bf16),
             jax.ShapeDtypeStruct((hidden, width), bf16),
-            jax.ShapeDtypeStruct((8, width // ep_count), f32),
+            jax.ShapeDtypeStruct((8, seg), f32),
         ),
-        in_specs=[anywhere, anywhere, vmem, vmem, anywhere, anywhere, anywhere],
+        in_specs=[hbm] * 7,
         out_specs=[vmem] * 6,
         scratch_shapes=[
             pltpu.VMEM((2, tok_rows, width), bf16),
@@ -598,25 +622,28 @@
             pltpu.VMEM((LINE,) + tiny, f32),
             pltpu.VMEM((ep_count,) + tiny, f32),
             pltpu.VMEM((total, 128), f32),
+            pltpu.VMEM((routes.shape[1], tok_rows), jnp.int32),
+            pltpu.VMEM((experts, width), bf16),
+            pltpu.VMEM((8, width), f32),
             pltpu.VMEM((total, hidden), bf16),
             pltpu.VMEM((total, 2 * hidden), bf16),
             pltpu.VMEM((LINE, PLANES, pair, part), bf16),
             pltpu.VMEM((LINE, PLANES, pair, part), f32),
             pltpu.VMEM((LINE, PLANES, pair, part), bf16),
-            pltpu.VMEM((LINE, BLOCKS, cap, part), bf16),
-            pltpu.VMEM((LINE, BLOCKS, cap, part), bf16),
-            pltpu.VMEM((LINE, BLOCKS, cap, part), f32),
-            pltpu.VMEM((LINE, cap, part), bf16),
-            pltpu.VMEM((LINE, cap, part), bf16),
+            pltpu.VMEM((LINE, 3, cap, part), bf16),
+            pltpu.VMEM((LINE, 3, cap, part), bf16),
+            pltpu.VMEM((LINE, cap, part), f32),
             pltpu.VMEM((LINE - 1, cap, part), bf16),
             pltpu.VMEM((LINE, cap, part), bf16),
             pltpu.VMEM(tiny, f32),
+            pltpu.VMEM((2,) + tiny, f32),
             pltpu.VMEM((4,) + tiny, f32),
-            pltpu.VMEM((3,) + tiny, f32),
             pltpu.VMEM((LINE,) + tiny, f32),
-            pltpu.VMEM((8, width), f32),
-            pltpu.VMEM((ep_count, 8, width // ep_count), f32),
-            dma((5,)),
+            pltpu.VMEM((BLOCKS, LINE, 8, wide), f32),
+            pltpu.VMEM((LINE, 8, wide), f32),
+            pltpu.VMEM((LINE, 8, wide), f32),
+            pltpu.VMEM((LINE - 1, 8, wide), f32),
+            dma((7,)),
             dma((2, LINE, PIECES)),
             dma((2, LINE, PIECES)),
             dma((2, LINE, BLOCKS, PIECES)),
@@ -624,25 +651,43 @@
             dma((2, LINE)),
             dma((2, LINE)),
             dma((2, LINE, PLANES)),
-            dma((2, LINE, BLOCKS)),
+            dma((2, LINE, 3)),
+            dma((2, LINE)),
+            dma((2, 4)),
             dma((2, LINE)),
             dma((2, LINE)),
-            dma((2, 3)),
-            dma((2, LINE)),
-            dma((2, ep_count)),
         ],
         compiler_params=pltpu.CompilerParams(
-            collective_id=0, has_side_effects=True, vmem_limit_bytes=60 * 1024 * 1024
+            collective_id=0, has_side_effects=True, vmem_limit_bytes=VMEM_LIMIT
         ),
-    )(tokens, cotangent, routes_t, router_t, w_gate[0], w_up[0], w_down[0])
-    own = lax.dynamic_slice_in_dim(router_grad, lax.axis_index("tp") * seg, seg, 1)
+    )(*map(in_hbm, (tokens, cotangent, routes.T, router.T, w_gate[0], w_up[0], w_down[0])))
+    top = routes.shape[1]
+    token_grad, gates, grad_gate, grad_up, grad_down, router_grad = pl.pallas_call(
+        store_kernel,
+        out_shape=(
+            jax.ShapeDtypeStruct((tok_rows, part), bf16),
+            jax.ShapeDtypeStruct((top, tok_rows), f32),
+            jax.ShapeDtypeStruct((width, hidden), bf16),
+            jax.ShapeDtypeStruct((width, hidden), bf16),
+            jax.ShapeDtypeStruct((hidden, width), bf16),
+            jax.ShapeDtypeStruct((experts, seg), f32),
+        ),
+        in_specs=[vmem] * 6,
+        out_specs=[hbm] * 6,
+        scratch_shapes=[
+            pltpu.VMEM((top, tok_rows), f32),
+            pltpu.VMEM((experts, seg), f32),
+            dma((6,)),
+        ],
+        compiler_params=pltpu.CompilerParams(vmem_limit_bytes=16 * 1024 * 1024),
+    )(*results)
     return (
         token_grad,
-        gates[: routes.shape[1]].T,
+        gates.T,
         grad_gate[None],
         grad_up[None],
         grad_down[None],
-        own[:experts].T,
+        router_grad.T,
     )
 
 

time: 98.9 us -> 75 us (0.76)
  local copies, waits for them, and re-layouts: 12.3 us -> 0 us
  Pallas kernels: 84.2 us -> 74 us
  other arithmetic: 1.35 us -> 0 us
    pallas_call x1, Pallas kernels: 84.2 us -> 71.3 us  [fused_shards(): pl.pallas_call(fused_kernel, out_shape=(jax.ShapeDtypeStruct((tok_rows, p...]
    unnamed x8 -> x0, local copies, waits for them, and re-layouts: 8.43 us -> none
    pallas_call x0 -> x1, Pallas kernels: none -> 2.76 us  [fused_shards(): pl.pallas_call(store_kernel, out_shape=(jax.ShapeDtypeStruct((tok_rows, p...]
    transpose x2 -> x0, local copies, waits for them, and re-layouts: 1.83 us -> none  [the longest x1 1.25 us: fused_shards(): gates[:routes.shape[1]]]
    pad x1 -> x0, other arithmetic: 1.35 us -> none  [fused_shards(): router_t = jnp.pad(router.T.astype(jnp.float32), ((0, 8 - experts), (0, 0)))]
    pad x1 -> x0, local copies, waits for them, and re-layouts: 1.28 us -> none  [fused_shards(): routes_t = jnp.pad(routes.T, ((0, 8 - routes.shape[1]), (0, 0)))]
where the time goes in v2:
time: 75 us; the launch traced here: 74.8 us
  Pallas kernels  74 us (99%)
  between operations  0.8 us (1%)
    pallas_call x1, Pallas kernels, fused_shards(): pl.pallas_call(fused_kernel, out_shape=(jax.ShapeDtypeStruct((tok_rows, p...  71.3 us
    pallas_call x1, Pallas kernels, fused_shards(): pl.pallas_call(store_kernel, out_shape=(jax.ShapeDtypeStruct((tok_rows, p...  2.76 us

profile of v2, /device:TPU:0, one launch (start us, length us, event | category | flops | bytes accessed | tf_op | source)
XLA Modules:
  0.0 74.8 jit_solution(7426111391389916333)
XLA Ops:
  0.6 71.3 %shard_map.118 = (bf16[128,512]{1,0:T(8,128)(2,1)S(1)}, f32[8,128]{1,0:T(8,128)S(1)}, bf16[2048,512]{1,0:T(8,128)(2,1)S(1)}, bf16[2048,512]{1,0:T(8,128)(2,1)S(1...) custom-call(bf16[128,2048]{1,0:T(8,128)(2,1)} %tok_hbm.1, bf16[128,2048]{1,0:T(8,128)(2,1)} %cot_hbm.1, ...), custom_call_target="tpu_custom_call" | custom-call | tf_op jit(solution)/shard_map/pallas_call | solution.py:603
  71.9 2.8 %shard_map.119 = (bf16[128,512]{1,0:T(8,128)(2,1)}, f32[2,128]{1,0:T(2,128)}, bf16[2048,512]{1,0:T(8,128)(2,1)}, bf16[2048,512]{1,0:T(8,128)(2,1)}, bf16[512,2048]{1,0:T(8,128)(2,1)}, /*index=5*/f32[4,64]{1,0:T(4,128)}) custom-call(bf16[128,512]{1,0:T(8,128)(2,1)S(1)} %get-tuple-element.18.tg_in, f32[8,128]{1,0:T(8,128)S(1)} %get-tuple-element.19.gg_in, ...), custom_call_target="tpu_custom_call" | custom-call | tf_op jit(solution)/shard_map/pallas_call | solution.py:665

commit v3 on v2

--- a/solution.py
+++ b/solution.py
@@ -9,8 +9,8 @@
 CORES = 2
 PLANES = 2
 LINE = 4
-PIECES = 2
-SIXTEENTHS = 10
+PIECES = 1
+SIXTEENTHS = 9
 VMEM_LIMIT = 40 * 1024 * 1024
 MESH = pl.DeviceIdType.MESH
 
@@ -209,11 +209,9 @@
 
 
 SCHEDULE = (
-    "X00", "Z10", "Z11", "X01", "X10", "Z20", "Y010", "Y011", "X11", "Z21", "X20", "Z30", "F0",
-    "Y101", "X21", "D0", "Y110", "Z31", "Y201", "Y100", "A0", "Y111", "Y211", "Y200", "F1",
-    "X30", "X31", "Y210", "Y300", "D1", "F2", "Y301", "A1", "D2", "Y310", "Y311", "A2", "F3",
-    "G0", "D3", "E0", "E1", "G1", "A3", "W0", "G2", "E2", "W1", "E3", "G3", "R0", "W2", "T",
-    "R1",
+    "X00", "Z10", "X10", "Y010", "Z20", "F0", "D0", "X20", "Y110", "Y100", "Z30", "Y200", "F1",
+    "Y210", "D1", "X30", "F2", "D2", "A1", "Y300", "A2", "Y310", "F3", "D3", "G0", "G1", "A3",
+    "W0", "E1", "W1", "E2", "R0", "W2", "G2", "R1", "A0", "E3", "G3", "R2", "E0", "T", "R3",
 )
 
 
@@ -222,7 +220,7 @@
     tg_ref, gg_ref, gw_ref, gu_ref, gd_ref, rg_ref,
     src, wgu, wd, rows, pack, hot, gate_send, gate_recv, gate_col,
     routes_ref, router_ref, router_all, hs, dgu, dx_send, dx_own, c_recv, s_send, s_recv, s_own, z_send, z_recv,
-    g_sum, g_send, g_recv, gz_recv, r_send, r_recv, rz_send, rz_recv,
+    g_sum, g_send, g_recv, gz_recv, coefs, term_col, r_send, r_core, r_sum, r_recv, rz_send, rz_recv,
     load_sems, z_sems, x_sems, y_sems, c_sems, gz_sems, gx_sems,
     sc_sems, s_sems, sz_sems, gp_sems, gl_sems, r_sems,
 ):
@@ -256,6 +254,11 @@
         ).wait_recv()
 
     greeted = at.announce()
+    def thirds(value):
+        high = value.astype(bf16).astype(f32)
+        middle = (value - high).astype(bf16).astype(f32)
+        return [high, middle, (value - high - middle).astype(bf16).astype(f32)]
+
     loads = [
         pltpu.make_async_copy(routes_hbm, routes_ref, load_sems.at[5]),
         pltpu.make_async_copy(tok_hbm, src.at[0], load_sems.at[0]),
@@ -314,14 +317,13 @@
     pl.semaphore_wait(pltpu.get_barrier_semaphore(), greeted)
     for h in range(PIECES):
         pass_x(0, h)
-    for m in range(LINE - 1):
-        for h in range(PIECES):
-            begin = pl.multiple_of(at.slots[m] * BLOCKS * cap + h * size, 16)
-            send(
-                pack.at[m, pl.ds(h * size, size), :],
-                rows.at[at.c, pl.ds(begin, size), window],
-                z_sems.at[0, m, h], z_sems.at[1, at.slots[m], h], at.along(at.lines[m]),
-            )
+    order = [(m, h) for m in range(LINE - 1) for h in range(PIECES)]
+    for m, h in order:
+        begin = pl.multiple_of(at.slots[m] * BLOCKS * cap + h * size, 16)
+        send(
+            pack.at[m, pl.ds(h * size, size), :], rows.at[at.c, pl.ds(begin, size), window],
+            z_sems.at[0, m, h], z_sems.at[1, at.slots[m], h], at.along(at.lines[m]),
+        )
 
     experts = router_ref.shape[0]
     loads[3].wait()
@@ -336,6 +338,9 @@
     weights = [jax.nn.sigmoid(margin), jax.nn.sigmoid(-margin)]
     sent = [w.astype(bf16).astype(f32) for w in weights]
     by_expert = jnp.where(is_first, sent[0], 0.0) + jnp.where(is_second, sent[1], 0.0)
+    notes = [(first + second).astype(f32)] + thirds(weights[0] * weights[1])
+    for n, note in enumerate(notes):
+        by_expert = jnp.where(row8 == LINE + n, note, by_expert)
     for m, z in enumerate((at.z,) + at.lines):
         gate_send[m] = dot(by_expert.astype(bf16), hot[z], ((1,), (1,)))
     gate_recv[0] = gate_send[0]
@@ -405,6 +410,7 @@
         dgu[chunk(k), 0:hidden] = (scaled * pre_up * sig * (1.0 + pre_gate * (1.0 - sig))).astype(bf16)
         dgu[chunk(k), hidden:] = (scaled * active).astype(bf16)
         hs[chunk(k), :] = (gate * product).astype(bf16)
+        term_col[chunk(k), :] = jnp.broadcast_to(terms, (BLOCKS * cap, side))
         for j in range(BLOCKS):
             line = jnp.sum(
                 jnp.where(diagonal[0:cap], terms[j * cap : (j + 1) * cap], 0.0),
@@ -487,10 +493,7 @@
     state = {}
 
     def split3(value):
-        high = value.astype(bf16).astype(f32)
-        middle = (value - high).astype(bf16).astype(f32)
-        low = (value - high - middle).astype(bf16).astype(f32)
-        return jnp.concatenate([high, middle, low, jnp.zeros_like(value)], axis=0).astype(bf16)
+        return jnp.concatenate(thirds(value) + [jnp.zeros_like(value)], axis=0).astype(bf16)
 
     def gate_finish():
         for m in range(LINE - 1):
@@ -506,14 +509,6 @@
         lead = weights[0] * weights[1] * (grads[0] - grads[1])
         logit_grad = jnp.where(is_first, lead, 0.0) - jnp.where(is_second, lead, 0.0)
         state["parts"] = split3(logit_grad)
-        sums = dot(state["parts"], src[0], ((1,), (0,)))
-        sums = sums[0:8] + sums[8:16] + sums[16:24]
-        wide = r_send.shape[3]
-        for z in range(LINE):
-            for x in range(BLOCKS):
-                begin = (z * BLOCKS + x) * wide
-                r_send[x, z] = sums[:, begin : begin + wide]
-        send(r_send.at[1 - at.x], r_recv, r_sems.at[0, 0], r_sems.at[1, 0], at.across())
 
     def token_finish():
         begin = pl.multiple_of(at.tp * part, part)
@@ -528,17 +523,51 @@
 
     def router_stage(n):
         if n == 0:
-            arrived(r_recv, r_sems.at[1, 0])
-            rz_send[...] = r_send[at.x] + r_recv[...]
+            lanes = lax.broadcasted_iota(jnp.int32, (cap, side), 1)
+            expert = lanes % 8
+            for b in range(LINE * BLOCKS):
+                notes = gate_recv[b]
+                other = to_column(notes[4:5])[0:cap].astype(jnp.int32) - at.z
+                lead = to_column(notes[5:6] + notes[6:7] + notes[7:8])[0:cap]
+                lead = lead * term_col[b * cap : (b + 1) * cap, :]
+                lead = jnp.where(expert == at.z, lead, jnp.where(expert == other, -lead, 0.0))
+                high, middle, low = thirds(lead)
+                coefs[b * cap : (b + 1) * cap, :] = jnp.where(
+                    lanes < 8, high, jnp.where(lanes < 16, middle, jnp.where(lanes < 24, low, 0.0))
+                ).astype(bf16)
+            sums = dot(coefs[...], rows[0], ((0,), (0,)))
+            sums = sums[0:8] + sums[8:16] + sums[16:24]
+            wide = r_send.shape[3]
+            for z in range(LINE):
+                for x in range(BLOCKS):
+                    begin = (z * BLOCKS + x) * wide
+                    r_send[x, z] = sums[:, begin : begin + wide]
+            send(r_send, r_core, r_sems.at[0, 0], r_sems.at[1, 0], at.other_core())
+            return
+        if n == 1:
+            arrived(r_core, r_sems.at[1, 0])
+            r_sum[...] = r_send[...] + r_core[...]
+            ways = ((1 - at.x, at.across), (at.x, at.other_plane), (1 - at.x, at.diagonal))
+            for i, (x, peer) in enumerate(ways):
+                send(
+                    r_sum.at[x], r_recv.at[i], r_sems.at[0, 1 + i], r_sems.at[1, 1 + i], peer()
+                )
+            return
+        if n == 2:
+            total = r_sum[at.x]
+            for i in range(3):
+                arrived(r_recv.at[i], r_sems.at[1, 1 + i])
+                total = total + r_recv[i]
+            rz_send[...] = total
             for m in range(LINE - 1):
                 send(
                     rz_send.at[at.lines[m]], rz_recv.at[at.slots[m] - 1],
-                    r_sems.at[0, m + 1], r_sems.at[1, at.slots[m]], at.along(at.lines[m]),
+                    r_sems.at[0, m + 4], r_sems.at[1, at.slots[m] + 3], at.along(at.lines[m]),
                 )
             return
         total = rz_send[at.z]
         for m in range(LINE - 1):
-            arrived(rz_recv.at[m], r_sems.at[1, m + 1])
+            arrived(rz_recv.at[m], r_sems.at[1, m + 4])
             total = total + rz_recv[m]
         seg = rg_ref.shape[1]
         own = jnp.zeros((8, seg), f32)
@@ -639,8 +668,12 @@
             pltpu.VMEM((2,) + tiny, f32),
             pltpu.VMEM((4,) + tiny, f32),
             pltpu.VMEM((LINE,) + tiny, f32),
+            pltpu.VMEM((total, 128), bf16),
+            pltpu.VMEM((total, 128), f32),
             pltpu.VMEM((BLOCKS, LINE, 8, wide), f32),
-            pltpu.VMEM((LINE, 8, wide), f32),
+            pltpu.VMEM((BLOCKS, LINE, 8, wide), f32),
+            pltpu.VMEM((BLOCKS, LINE, 8, wide), f32),
+            pltpu.VMEM((3, LINE, 8, wide), f32),
             pltpu.VMEM((LINE, 8, wide), f32),
             pltpu.VMEM((LINE - 1, 8, wide), f32),
             dma((7,)),
@@ -655,7 +688,7 @@
             dma((2, LINE)),
             dma((2, 4)),
             dma((2, LINE)),
-            dma((2, LINE)),
+            dma((2, 7)),
         ],
         compiler_params=pltpu.CompilerParams(
             collective_id=0, has_side_effects=True, vmem_limit_bytes=VMEM_LIMIT

time: 75 us -> 71.7 us (0.956)
  Pallas kernels: 74 us -> 70.7 us
    pallas_call x1, Pallas kernels: 71.3 us -> 67.9 us  [fused_shards(): pl.pallas_call(fused_kernel, out_shape=(jax.ShapeDtypeStruct((tok_rows, p...]
where the time goes in v3:
time: 71.7 us; the launch traced here: 71.5 us
  Pallas kernels  70.7 us (99%)
  between operations  0.8 us (1%)
    pallas_call x1, Pallas kernels, fused_shards(): pl.pallas_call(fused_kernel, out_shape=(jax.ShapeDtypeStruct((tok_rows, p...  67.9 us
    pallas_call x1, Pallas kernels, fused_shards(): pl.pallas_call(store_kernel, out_shape=(jax.ShapeDtypeStruct((tok_rows, p...  2.76 us

profile of v3, /device:TPU:0, one launch (start us, length us, event | category | flops | bytes accessed | tf_op | source)
XLA Modules:
  0.0 71.5 jit_solution(2227045631017945961)
XLA Ops:
  0.6 67.9 %shard_map.118 = (bf16[128,512]{1,0:T(8,128)(2,1)S(1)}, f32[8,128]{1,0:T(8,128)S(1)}, bf16[2048,512]{1,0:T(8,128)(2,1)S(1)}, bf16[2048,512]{1,0:T(8,128)(2,1)S(1...) custom-call(bf16[128,2048]{1,0:T(8,128)(2,1)} %tok_hbm.1, bf16[128,2048]{1,0:T(8,128)(2,1)} %cot_hbm.1, ...), custom_call_target="tpu_custom_call" | custom-call | tf_op jit(solution)/shard_map/pallas_call | solution.py:632
  68.6 2.8 %shard_map.119 = (bf16[128,512]{1,0:T(8,128)(2,1)}, f32[2,128]{1,0:T(2,128)}, bf16[2048,512]{1,0:T(8,128)(2,1)}, bf16[2048,512]{1,0:T(8,128)(2,1)}, bf16[512,2048]{1,0:T(8,128)(2,1)}, /*index=5*/f32[4,64]{1,0:T(4,128)}) custom-call(bf16[128,512]{1,0:T(8,128)(2,1)S(1)} %get-tuple-element.18.tg_in, f32[8,128]{1,0:T(8,128)S(1)} %get-tuple-element.19.gg_in, ...), custom_call_target="tpu_custom_call" | custom-call | tf_op jit(solution)/shard_map/pallas_call | solution.py:698
